TPU v7x, 768 devices: a whole 4x8x12 slice. The times are simulated.
768 devices in a mesh: fs: 12 (over z), rep: 8 (over y), tp: 8 (over x, core).
Axes of the slice: x: 4, y: 8, z: 12, core: 2. Of those that a mesh axis runs over, the one named last changes fastest.
Arguments:
- saved_input: bfloat16 [61440, 3072], P(('fs', 'rep')), may hold values from -20 to 20
- key_cotangent: bfloat16 [61440, 1024], P(('fs', 'rep'), 'tp'), may hold values from -0.015625 to 0.015625
- value_cotangent: bfloat16 [61440, 2048], P(('fs', 'rep'), 'tp'), may hold values from -0.015625 to 0.015625
- key_factor: bfloat16 [3072, 256], replicated, may hold values from -0.375 to 0.375
- value_factor: bfloat16 [3072, 256], replicated, may hold values from -0.375 to 0.375
- key_weight: float32 [3072, 1024], P(('fs', 'rep'), 'tp'), may hold values from -0.109375 to 0.109375
- value_weight: float32 [3072, 2048], P(('fs', 'rep'), 'tp'), may hold values from -0.109375 to 0.109375
- key_first: float32 [256, 1024], P(None, 'tp'), as said below
- key_second: float32 [256, 1024], P(None, 'tp'), may hold values from 0.05 to 1
- value_first: float32 [256, 2048], P(None, 'tp'), as said below
- value_second: float32 [256, 2048], P(None, 'tp'), may hold values from 0.05 to 1
Outputs:
- key_weight_new: float32 [3072, 1024], P(('fs', 'rep'), 'tp')
- value_weight_new: float32 [3072, 2048], P(('fs', 'rep'), 'tp')
- key_first_new: float32 [256, 1024], P(None, 'tp')
- key_second_new: float32 [256, 1024], P(None, 'tp')
- value_first_new: float32 [256, 2048], P(None, 'tp')
- value_second_new: float32 [256, 2048], P(None, 'tp')
- key_step: float32 [3072, 1024], P(('fs', 'rep'), 'tp')
- value_step: float32 [3072, 2048], P(('fs', 'rep'), 'tp')
- key_copy: bfloat16 [3072, 1024], P(None, 'tp')
- value_copy: bfloat16 [3072, 2048], P(None, 'tp')
Inputs may be any that keep to these rules, and one draw needn't show every extreme that they name: `key_first`: real-valued moments whose scale differs from head to head. `value_first`: real-valued moments whose scale differs from head to head.
All inputs are finite; a program needn't handle non-finite values.
Results may differ from a plain program's by a relative error of at most 0.004.
Values may be sent and summed in bfloat16 or wider, within the bound.
A program may use at most 64 MiB of HBM per device.

v0:
```python
import jax
import jax.numpy as jnp
from jax import lax
from jax.sharding import PartitionSpec as P

DK = 1024
DV = 2048
RK = 256
RV = 256


first_decay = 0.8
second_decay = 0.9
epsilon = 1e-08
learn_rate = 0.01


def in_one(arrays, axis):
    vector, at, outs = (jnp.concatenate([a.reshape(-1) for a in arrays]), 0, [])
    total = lax.psum(vector, axis)
    for a in arrays:
        outs.append(total[at : at + a.size].reshape(a.shape))
        at += a.size
    return tuple(outs)


def gathered_total(x, axis):
    return lax.all_gather(x, axis).sum(0)


def laid_out(pieces, dim):
    dims = list(pieces.shape[1:])
    dims[dim] *= pieces.shape[0]
    return jnp.moveaxis(pieces, 0, dim).reshape(dims)


def stacked_from(x, axes, order):
    pieces = x[None]
    for k in order:
        pieces = lax.all_gather(pieces, axes[k], axis=0, tiled=True)
    block = [lax.axis_size(axes[k]) for k in reversed(order)]
    pieces = pieces.reshape(*block, *x.shape)
    turned = sorted(range(len(order)), key=lambda place: order[len(order) - 1 - place])
    return pieces.transpose(*turned, *range(len(order), pieces.ndim)).reshape(-1, *x.shape)


def whole_of(x, axes, order, dim):
    return laid_out(stacked_from(x, axes, order), dim)


def split_contract(basis, cotangent):
    upper = basis.astype(jnp.bfloat16)
    lower = (basis - upper.astype(jnp.float32)).astype(jnp.bfloat16)
    dims = (((0,), (0,)), ((), ()))
    high_part = lax.dot_general(upper, cotangent, dims, preferred_element_type=jnp.float32)
    low_part = lax.dot_general(lower, cotangent, dims, preferred_element_type=jnp.float32)
    return high_part + low_part


def moments(projection, first, second):
    first_new = first_decay * first + (1.0 - first_decay) * projection
    second_new = second_decay * second + (1.0 - second_decay) * projection * projection
    normed = first_new / (jnp.sqrt(second_new) + epsilon)
    return (first_new, second_new, normed)


def body(
    saved_input,
    key_cotangent,
    value_cotangent,
    key_factor,
    value_factor,
    key_weight,
    value_weight,
    key_first,
    key_second,
    value_first,
    value_second,
):
    local_rows = key_weight.shape[0]
    row_offset = lax.axis_index(("fs", "rep")) * local_rows
    key_rows = lax.dynamic_slice_in_dim(key_factor, row_offset, local_rows, 0).astype(jnp.float32)
    value_rows = lax.dynamic_slice_in_dim(value_factor, row_offset, local_rows, 0).astype(
        jnp.float32
    )
    key_basis = jnp.dot(saved_input, key_factor, preferred_element_type=jnp.float32)
    key_part = split_contract(key_basis, key_cotangent)
    value_basis = jnp.dot(saved_input, value_factor, preferred_element_type=jnp.float32)
    value_part = split_contract(value_basis, value_cotangent)
    key_projected, value_projected = in_one((key_part, value_part), ("fs", "rep"))
    key_first_new, key_second_new, key_normed = moments(key_projected, key_first, key_second)
    value_first_new, value_second_new, value_normed = moments(
        value_projected, value_first, value_second
    )
    local_squares = jnp.sum(key_normed * key_normed) + jnp.sum(value_normed * value_normed)
    squares = gathered_total(local_squares, "tp")
    entries = jnp.float32(RK * DK + RV * DV)
    shrink = jnp.sqrt(entries / (entries + squares))
    key_step = shrink * jnp.dot(key_rows, key_normed, precision=lax.Precision.HIGHEST)
    value_step = shrink * jnp.dot(value_rows, value_normed, precision=lax.Precision.HIGHEST)
    key_weight_new = key_weight - learn_rate * key_step
    value_weight_new = value_weight - learn_rate * value_step
    key_copy, value_copy = (
        whole_of(key_weight_new.astype(jnp.bfloat16), ("fs", "rep"), (0, 1), 0),
        whole_of(value_weight_new.astype(jnp.bfloat16), ("fs", "rep"), (0, 1), 0),
    )
    return (
        key_weight_new,
        value_weight_new,
        key_first_new,
        key_second_new,
        value_first_new,
        value_second_new,
        key_step,
        value_step,
        key_copy,
        value_copy,
    )


def solution(mesh):
    in_specs = (
        P(("fs", "rep"), None),
        P(("fs", "rep"), "tp"),
        P(("fs", "rep"), "tp"),
        P(),
        P(),
        P(("fs", "rep"), "tp"),
        P(("fs", "rep"), "tp"),
        P(None, "tp"),
        P(None, "tp"),
        P(None, "tp"),
        P(None, "tp"),
    )
    out_specs = (
        P(("fs", "rep"), "tp"),
        P(("fs", "rep"), "tp"),
        P(None, "tp"),
        P(None, "tp"),
        P(None, "tp"),
        P(None, "tp"),
        P(("fs", "rep"), "tp"),
        P(("fs", "rep"), "tp"),
        P(None, "tp"),
        P(None, "tp"),
    )
    return jax.shard_map(body, mesh=mesh, in_specs=in_specs, out_specs=out_specs, check_vma=False)
```

profile of v0, /device:TPU:16, one launch (start us, length us, event | category | flops | bytes accessed | tf_op | source)
XLA Modules:
  0.0 355.2 jit_solution(12001802743386273043)
XLA Ops:
  7.3 3.9 %fusion.18 = f32[640,256]{1,0:T(8,128)S(1)} fusion(bf16[640,3072]{1,0:T(8,128)(2,1)} %param.11, bf16[3072,256]{1,0:T(8,128)(2,1)} %param.14), kind=kOutput, calls=%fused_computation.34 | convolution fusion | flops 1006632960 | bytes 6160384 | tf_op jit(solution)/shard_map/dot_general | solution.py:86
  11.2 0.3 fusion.7
  11.5 0.3 fusion.1
  11.8 1.2 fusion.19
  13.0 0.3 fusion.4
  13.4 0.3 fusion
  13.7 0.1 copy.25
  13.8 0.8 pad_maximum_fusion
  14.7 1.3 dynamic-slice
  16.0 234.0 %all-reduce.3.cloned.1.call-done = f32[98304]{0:T(1024)} async-done(((f32[98304]{0:T(1024)}), f32[98304]{0:T(1024)}) %all-reduce.3.cloned.1.call-update) | async-done | bytes 393232 | tf_op jit(solution)/shard_map/psum | solution.py:20
  250.0 1.0 slice.31
  251.0 0.1 slice.29
  251.1 0.8 multiply_reduce_fusion
  251.9 1.7 multiply_reduce_fusion.1
  254.9 0.8 dynamic-update-slice
  255.7 12.4 %all-reduce = f32[8]{0:T(128)S(1)} all-reduce(f32[8]{0:T(128)S(1)} %dynamic-update-slice), channel_id=1, replica_groups=mesh['fs'=12,'rep'=8,'tp'=8] {'tp'}, use_global_device_ids=true, to_apply=%add | all-reduce | flops 8 | bytes 64
  268.1 0.6 reduce_sum.29
  269.4 0.9 fusion.14
  270.4 23.9 %all-gather.1 = bf16[384,256]{1,0:T(8,128)(2,1)} all-gather(bf16[32,256]{1,0:T(8,128)(2,1)S(1)} %get-tuple-element.10), channel_id=3, replica_groups=mesh['fs'=12,'rep'=8,'tp'=8] {'fs'}, dimensions={0}, use_global_device_ids=true | all-gather | bytes 212992 | tf_op jit(solution)/shard_map/all_gather | solution.py:40
  294.3 1.6 fusion.15
  295.9 20.5 %all-gather = bf16[384,128]{1,0:T(8,128)(2,1)S(1)} all-gather(bf16[32,128]{1,0:T(8,128)(2,1)S(1)} %get-tuple-element.12), channel_id=2, replica_groups=mesh['fs'=12,'rep'=8,'tp'=8] {'fs'}, dimensions={0}, use_global_device_ids=true | all-gather | bytes 106496 | tf_op jit(solution)/shard_map/all_gather | solution.py:40
  316.4 28.3 %all_gather.21 = bf16[96,32,128]{2,1,0:T(8,128)(2,1)S(1)} all-gather(bf16[12,32,128]{2,1,0:T(8,128)(2,1)S(1)} %bitcast.39), channel_id=1, replica_groups=mesh['fs'=12,'rep'=8,'tp'=8] {'rep'}, dimensions={0}, use_global_device_ids=true | all-gather | bytes 884736 | tf_op jit(solution)/shard_map/all_gather | solution.py:40
  344.7 1.0 copy.23
  345.7 2.7 copy.24
  (34 shorter events, 0.2 us)
Async XLA Ops:
  7.2 4.6 %copy-start = (bf16[3072,256]{1,0:T(8,128)(2,1)S(1)}, bf16[3072,256]{1,0:T(8,128)(2,1)}, u32[]{:S(2)}) copy-start(bf16[3072,256]{1,0:T(8,128)(2,1)} %param.15) | copy-start | bytes 4718596
  7.2 4.0 %copy-start.2 = (bf16[640,128]{1,0:T(8,128)(2,1)S(1)}, bf16[640,128]{1,0:T(8,128)(2,1)}, u32[]{:S(2)}) copy-start(bf16[640,128]{1,0:T(8,128)(2,1)} %param.12) | copy-start | bytes 491524
  7.2 242.8 %all-reduce.3.cloned.1.call-start = ((), (), s32[]{:S(2)}) async-start(), calls=%async_computation | async-start | bytes 786432 | tf_op jit(solution)/shard_map/psum | solution.py:20
  7.2 4.6 %copy-start.11 = (bf16[640,3072]{1,0:T(8,128)(2,1)S(1)}, bf16[640,3072]{1,0:T(8,128)(2,1)}, u32[]{:S(2)}) copy-start(bf16[640,3072]{1,0:T(8,128)(2,1)} %param.11) | copy-start | bytes 11796484
  11.8 1.2 copy-start.1
  13.7 237.4 %copy-start.3 = (f32[256,256]{1,0:T(8,128)S(1)}, f32[256,256]{1,0:T(8,128)}, u32[]{:S(2)}) copy-start(f32[256,256]{1,0:T(8,128)} %param.21) | copy-start | bytes 786436
  13.7 237.4 %copy-start.4 = (f32[256,256]{1,0:T(8,128)S(1)}, f32[256,256]{1,0:T(8,128)}, u32[]{:S(2)}) copy-start(f32[256,256]{1,0:T(8,128)} %param.20) | copy-start | bytes 786436
  14.6 237.2 %copy-start.7 = (f32[256,128]{1,0:T(8,128)S(1)}, f32[256,128]{1,0:T(8,128)}, u32[]{:S(2)}) copy-start(f32[256,128]{1,0:T(8,128)} %param.19) | copy-start | bytes 393220
  14.6 237.2 %copy-start.8 = (f32[256,128]{1,0:T(8,128)S(1)}, f32[256,128]{1,0:T(8,128)}, u32[]{:S(2)}) copy-start(f32[256,128]{1,0:T(8,128)} %param.18) | copy-start | bytes 393220
  14.6 254.8 %copy-start.12 = (f32[32,256]{1,0:T(8,128)S(1)}, f32[32,256]{1,0:T(8,128)}, u32[]{:S(2)}) copy-start(f32[32,256]{1,0:T(8,128)} %param.17) | copy-start | bytes 98308
  14.7 331.0 %all-gather.4.cloned.1.call-start = ((), (), s32[]{:S(2)}) async-start(), calls=%async_computation.1 | async-start | bytes 1769472 | tf_op jit(solution)/shard_map/all_gather | solution.py:40
  251.1 43.2 %copy-start.13 = (f32[32,128]{1,0:T(8,128)S(1)}, f32[32,128]{1,0:T(8,128)}, u32[]{:S(2)}) copy-start(f32[32,128]{1,0:T(8,128)} %param.16) | copy-start | bytes 49156
  251.9 92.8 %copy-start.5 = (f32[256,256]{1,0:T(8,128)}, f32[256,256]{1,0:T(8,128)S(1)}, u32[]{:S(2)}) copy-start(f32[256,256]{1,0:T(8,128)S(1)} %get-tuple-element.15) | copy-start | bytes 786436
  251.9 92.8 %copy-start.6 = (f32[256,256]{1,0:T(8,128)}, f32[256,256]{1,0:T(8,128)S(1)}, u32[]{:S(2)}) copy-start(f32[256,256]{1,0:T(8,128)S(1)} %get-tuple-element.16) | copy-start | bytes 786436
  253.6 92.0 %copy-start.9 = (f32[256,128]{1,0:T(8,128)}, f32[256,128]{1,0:T(8,128)S(1)}, u32[]{:S(2)}) copy-start(f32[256,128]{1,0:T(8,128)S(1)} %get-tuple-element.18) | copy-start | bytes 393220
  253.6 92.0 %copy-start.10 = (f32[256,128]{1,0:T(8,128)}, f32[256,128]{1,0:T(8,128)S(1)}, u32[]{:S(2)}) copy-start(f32[256,128]{1,0:T(8,128)S(1)} %get-tuple-element.19) | copy-start | bytes 393220
Sparse Core Ops, SparseCore 0:
  14.8 235.1 all-reduce.2
  294.4 38.3 all-gather.3
where the time goes:
time: 356 us; the launch traced here: 355 us
  waiting for transfers between devices  234 us (66%)
  blocking collectives  85.1 us (24%)
  between operations  16.3 us (5%)
  matrix products  8.82 us (2%)
  local copies, waits for them, and re-layouts  6.96 us (2%)
  other arithmetic  3.89 us (1%)
    psum x1, waiting for transfers between devices, in_one(): total = lax.psum(vector, axis)  234 us
    all_gather x3, blocking collectives, stacked_from(): pieces = lax.all_gather(pieces, axes[k], axis=0, tiled=True)  72.7 us
    unnamed x1, blocking collectives  12.4 us
  transfers between devices with their start and end apart: 2, of which 1 were waited for; matrix products, arithmetic and copies ran while one was open for 1% of the time, Pallas kernels for 0%

commit v1 on v0

v1 whole, which is shorter than its diff:
```python
import jax
import jax.numpy as jnp
from jax import lax
from jax.experimental import pallas as pl
from jax.experimental.pallas import tpu as pltpu
from jax.sharding import PartitionSpec as P

MESH = pl.DeviceIdType.MESH
D, DK, DV, RK, RV = 3072, 1024, 2048, 256, 256
NZ, NY, NT = 12, 8, 8
TOK = 640
KC, VC = 128, 256
NC = KC + VC
ROWS = 32
KCHUNKS = 4
KSIZE = D // KCHUNKS

first_decay = 0.8
second_decay = 0.9
epsilon = 1e-08
learn_rate = 0.01


def kernel(
    x_hbm, ck_hbm, cv_hbm, fk_hbm, fv_hbm, wk_hbm, wv_hbm, m1k_hbm, m2k_hbm, m1v_hbm, m2v_hbm,
    wkn_hbm, wvn_hbm, m1kn_hbm, m2kn_hbm, m1vn_hbm, m2vn_hbm, sk_hbm, sv_hbm, kcopy_hbm, vcopy_hbm,
    xs, cs_k, cs_v, fk, fv, wk, wv, m1, m2, basis, part, rs1_send, rs1_recv, rs2_send, rs2_recv,
    ag, kg, vg, normed, acc, kout, vout, sq, sq_recv, ok, ov, osk, osv,
    in_sem, out_sem, r1s, r1r, r2s, r2r, a1s, a1r, a2s, a2r, k1s, k1r, v1s, v1r, krs, krr, vrs, vrr, ts, tr,
):
    z, y, t = lax.axis_index("fs"), lax.axis_index("rep"), lax.axis_index("tp")

    def zpeer(d):
        return (lax.rem(z + d, NZ), y, t)

    def ypeer(d):
        return (z, lax.rem(y + d, NY), t)

    def tpeer(d):
        return (z, y, lax.rem(t + d, NT))

    sends = []

    def send(src, dst, ssem, rsem, peer):
        copy = pltpu.make_async_remote_copy(
            src_ref=src, dst_ref=dst, send_sem=ssem, recv_sem=rsem, device_id=peer, device_id_type=MESH
        )
        copy.start()
        sends.append(copy)
        return copy

    def arrived(ref, ssem, rsem, peer):
        pltpu.make_async_remote_copy(
            src_ref=ref, dst_ref=ref, send_sem=ssem, recv_sem=rsem, device_id=peer, device_id_type=MESH
        ).wait_recv()

    loads = {}

    def load(name, src, dst):
        copy = pltpu.make_async_copy(src, dst, in_sem.at[len(loads)])
        copy.start()
        loads[name] = copy

    load("wk", wk_hbm, wk)
    load("wv", wv_hbm, wv)
    for c in range(KCHUNKS):
        ks = pl.ds(c * KSIZE, KSIZE)
        load(f"fk{c}", fk_hbm.at[ks], fk.at[ks])
        load(f"fv{c}", fv_hbm.at[ks], fv.at[ks])
        load(f"x{c}", x_hbm.at[:, ks], xs.at[:, ks])
    load("ck", ck_hbm, cs_k)
    load("cv", cv_hbm, cs_v)
    load("m1k", m1k_hbm, m1.at[0])
    load("m2k", m2k_hbm, m2.at[0])
    for c in range(2):
        cols = pl.ds(c * 128, 128)
        load(f"m1v{c}", m1v_hbm.at[:, cols], m1.at[1 + c])
        load(f"m2v{c}", m2v_hbm.at[:, cols], m2.at[1 + c])

    barrier = pltpu.get_barrier_semaphore()
    for d in range(1, NZ):
        pl.semaphore_signal(barrier, inc=1, device_id=zpeer(d), device_id_type=MESH)
    for d in range(1, NY):
        pl.semaphore_signal(barrier, inc=1, device_id=ypeer(d), device_id_type=MESH)
    for d in range(1, NT):
        pl.semaphore_signal(barrier, inc=1, device_id=tpeer(d), device_id_type=MESH)

    loads["wk"].wait()
    loads["wv"].wait()
    kg[z, y] = wk[...].astype(jnp.bfloat16)
    vg[z, y] = wv[...].astype(jnp.bfloat16)

    def basis_chunk(c):
        ks = slice(c * KSIZE, (c + 1) * KSIZE)
        for name in ("fk", "fv", "x"):
            loads[f"{name}{c}"].wait()
        xc = xs[:, ks]
        for f, cols in ((fk, slice(0, RK)), (fv, slice(RK, RK + RV))):
            term = jnp.dot(xc, f[ks, :], preferred_element_type=jnp.float32)
            if c == 0:
                basis[:, cols] = term
            else:
                basis[:, cols] += term

    basis_chunk(0)
    basis_chunk(1)

    pl.semaphore_wait(barrier, NZ - 1 + NY - 1 + NT - 1)
    for d in range(1, NY):
        send(vg.at[z, y], vg.at[z, y], v1s.at[d - 1], v1r.at[d - 1], ypeer(d))
    for d in range(1, NZ):
        send(kg.at[z, y], kg.at[z, y], k1s.at[d - 1], k1r.at[d - 1], zpeer(d))

    basis_chunk(2)
    basis_chunk(3)

    loads["ck"].wait()
    loads["cv"].wait()
    dims = (((0,), (0,)), ((), ()))
    for cols, cot, outs in (
        (slice(0, RK), cs_k, slice(0, KC)),
        (slice(RK, RK + RV), cs_v, slice(KC, NC)),
    ):
        b = basis[:, cols]
        upper = b.astype(jnp.bfloat16)
        lower = (b - upper.astype(jnp.float32)).astype(jnp.bfloat16)
        p = lax.dot_general(upper, cot[...], dims, preferred_element_type=jnp.float32)
        p += lax.dot_general(lower, cot[...], dims, preferred_element_type=jnp.float32)
        part[:, :, outs] = p.reshape(NY, ROWS, outs.stop - outs.start)
        rs1_send[:, :, outs] = p.reshape(NY, ROWS, outs.stop - outs.start).astype(jnp.bfloat16)

    for d in range(1, NY):
        peer = ypeer(d)
        send(rs1_send.at[peer[1]], rs1_recv.at[d - 1], r1s.at[d - 1], r1r.at[d - 1], peer)

    def half(c, n):
        return pl.ds(c * n, n)

    def kblock(owner, c):
        return kg.at[half(c, NZ // 2), owner]

    def vblock(owner, c):
        return vg.at[owner, half(c, NY // 2)]

    def ring(block, me, n, peer_of, ssem, rsem):
        steps = n // 2

        def owner_of(direction, hops):
            return lax.rem(me + (n - hops if direction == 0 else hops), n)

        def carries(direction, s, c):
            return s < steps or c == direction

        def put(direction, s, c):
            ref = block(owner_of(direction, s - 1), c)
            send(ref, ref, ssem.at[direction, s - 1, c], rsem.at[direction, s - 1, c],
                 peer_of(1 if direction == 0 else n - 1))

        def take(direction, s, c):
            ref = block(owner_of(direction, s), c)
            arrived(ref, ssem.at[direction, s - 1, c], rsem.at[direction, s - 1, c],
                    peer_of(1 if direction == 0 else n - 1))

        ticks = []
        for s in range(1, steps + 1):
            for c in range(2):
                for direction in range(2):
                    if not carries(direction, s, c):
                        continue

                    def tick(direction=direction, s=s, c=c):
                        take(direction, s, c)
                        if s < steps and carries(direction, s + 1, c):
                            put(direction, s + 1, c)

                    ticks.append(tick)

        def start():
            for c in range(2):
                for direction in range(2):
                    if carries(direction, 1, c):
                        put(direction, 1, c)

        return start, ticks

    vstart, vticks = ring(vblock, z, NZ, zpeer, vrs, vrr)
    kstart, kticks = ring(kblock, y, NY, ypeer, krs, krr)

    def run(ticks, count):
        for _ in range(min(count, len(ticks))):
            ticks.pop(0)()

    for d in range(1, NY):
        arrived(vg.at[z, lax.rem(y + NY - d, NY)], v1s.at[d - 1], v1r.at[d - 1], ypeer(d))
    vstart()
    for d in range(1, NZ):
        arrived(kg.at[lax.rem(z + NZ - d, NZ), y], k1s.at[d - 1], k1r.at[d - 1], zpeer(d))
    kstart()

    total = part[y]
    for d in range(1, NY):
        arrived(rs1_recv.at[d - 1], r1s.at[d - 1], r1r.at[d - 1], ypeer(d))
        total += rs1_recv[d - 1].astype(jnp.float32)
    for i in range(NZ):
        rs2_send[i] = total[8 * (i // 3) : 8 * (i // 3) + 8, 128 * (i % 3) : 128 * (i % 3) + 128]
    for d in range(1, NZ):
        peer = zpeer(d)
        send(rs2_send.at[peer[0]], rs2_recv.at[d - 1], r2s.at[d - 1], r2r.at[d - 1], peer)

    run(vticks, 4)
    run(kticks, 4)

    tile = rs2_send[z]
    for d in range(1, NZ):
        arrived(rs2_recv.at[d - 1], r2s.at[d - 1], r2r.at[d - 1], zpeer(d))
        tile += rs2_recv[d - 1]
    ag[y, z] = tile
    for d in range(1, NZ):
        send(ag.at[y, z], ag.at[y, z], a1s.at[d - 1], a1r.at[d - 1], zpeer(d))

    run(vticks, 4)
    run(kticks, 4)

    for d in range(1, NZ):
        arrived(ag.at[y, lax.rem(z + NZ - d, NZ)], a1s.at[d - 1], a1r.at[d - 1], zpeer(d))
    for d in range(1, NY):
        send(ag.at[y], ag.at[y], a2s.at[d - 1], a2r.at[d - 1], ypeer(d))

    run(vticks, 4)
    run(kticks, 4)
    run(vticks, 4)

    for d in range(1, NY):
        arrived(ag.at[lax.rem(y + NY - d, NY)], a2s.at[d - 1], a2r.at[d - 1], ypeer(d))

    outs = []

    def store(src, dst):
        copy = pltpu.make_async_copy(src, dst, out_sem.at[len(outs)])
        copy.start()
        outs.append(copy)

    squares = jnp.zeros((8, 128), jnp.float32)
    for g in range(3):
        for name in (("m1k", "m2k"), ("m1v0", "m2v0"), ("m1v1", "m2v1"))[g]:
            loads[name].wait()
        proj = jnp.concatenate([ag[b, 3 * i + g] for b in range(NY) for i in range(4)], axis=0)
        first_new = first_decay * m1[g] + (1.0 - first_decay) * proj
        second_new = second_decay * m2[g] + (1.0 - second_decay) * proj * proj
        m1[g] = first_new
        m2[g] = second_new
        n = first_new / (jnp.sqrt(second_new) + epsilon)
        squares += jnp.sum((n * n).reshape(RK // 8, 8, 128), axis=0)
        upper = n.astype(jnp.bfloat16)
        lower = (n - upper.astype(jnp.float32)).astype(jnp.bfloat16)
        normed[:, 128 * g : 128 * g + 128] = upper
        normed[:, NC + 128 * g : NC + 128 * g + 128] = lower
    sq[...] = squares
    for d in range(1, NT):
        send(sq, sq_recv.at[d - 1], ts.at[d - 1], tr.at[d - 1], tpeer(d))
    store(m1.at[0], m1kn_hbm)
    store(m2.at[0], m2kn_hbm)
    for c in range(2):
        cols = pl.ds(c * 128, 128)
        store(m1.at[1 + c], m1vn_hbm.at[:, cols])
        store(m2.at[1 + c], m2vn_hbm.at[:, cols])

    def rows_of(b):
        return pl.ds(pl.multiple_of(b * 256, 256), 256)

    @pl.loop(0, NZ)
    def _(b):
        rows = rows_of(b)
        wide = jnp.dot(
            fk[rows, :],
            jnp.concatenate([normed[:, 0:KC], normed[:, NC : NC + KC]], axis=1),
            preferred_element_type=jnp.float32,
        )
        acc[rows, 0:KC] = wide[:, :KC] + wide[:, KC:]
        acc[rows, KC:NC] = jnp.dot(
            fv[rows, :], normed[:, KC:NC], preferred_element_type=jnp.float32
        ) + jnp.dot(fv[rows, :], normed[:, NC + KC :], preferred_element_type=jnp.float32)

    run(vticks, 100)
    run(kticks, 100)

    squares = sq[...]
    for d in range(1, NT):
        arrived(sq_recv.at[d - 1], ts.at[d - 1], tr.at[d - 1], tpeer(d))
        squares += sq_recv[d - 1]
    whole = jnp.sum(jnp.sum(squares, axis=0, keepdims=True), axis=1, keepdims=True)
    entries = float(RK * DK + RV * DV)
    shrink = jnp.sqrt(entries / (entries + whole))

    mine = pl.ds(pl.multiple_of((z * NY + y) * ROWS, ROWS), ROWS)
    step_k = shrink * acc[mine, 0:KC]
    step_v = shrink * acc[mine, KC:NC]
    osk[...] = step_k
    osv[...] = step_v
    ok[...] = wk[...] - learn_rate * step_k
    ov[...] = wv[...] - learn_rate * step_v
    store(osk, sk_hbm)
    store(osv, sv_hbm)
    store(ok, wkn_hbm)
    store(ov, wvn_hbm)

    for b in range(NZ):
        rows = slice(b * 256, b * 256 + 256)
        kw = kg[b].reshape(256, KC).astype(jnp.float32)
        kout[rows, :] = (kw - learn_rate * (shrink * acc[rows, 0:KC])).astype(jnp.bfloat16)
        vw = vg[b].reshape(256, VC).astype(jnp.float32)
        vout[rows, :] = (vw - learn_rate * (shrink * acc[rows, KC:NC])).astype(jnp.bfloat16)
        store(kout.at[pl.ds(b * 256, 256)], kcopy_hbm.at[pl.ds(b * 256, 256)])
        store(vout.at[pl.ds(b * 256, 256)], vcopy_hbm.at[pl.ds(b * 256, 256)])

    for copy in sends:
        copy.wait_send()
    for copy in outs:
        copy.wait()


def body(*args):
    f32, bf16 = jnp.float32, jnp.bfloat16
    V, S = pltpu.VMEM, pltpu.SemaphoreType.DMA
    outs = [
        ((ROWS, KC), f32), ((ROWS, VC), f32), ((RK, KC), f32), ((RK, KC), f32), ((RV, VC), f32), ((RV, VC), f32),
        ((ROWS, KC), f32), ((ROWS, VC), f32), ((D, KC), bf16), ((D, VC), bf16),
    ]
    return pl.pallas_call(
        kernel,
        name="projected_update",
        out_shape=[jax.ShapeDtypeStruct(s, dt) for s, dt in outs],
        in_specs=[pl.BlockSpec(memory_space=pl.ANY)] * 11,
        out_specs=[pl.BlockSpec(memory_space=pl.ANY)] * 10,
        scratch_shapes=[
            V((TOK, D), bf16), V((TOK, KC), bf16), V((TOK, VC), bf16), V((D, RK), bf16), V((D, RV), bf16),
            V((ROWS, KC), f32), V((ROWS, VC), f32), V((3, RK, 128), f32), V((3, RK, 128), f32),
            V((TOK, RK + RV), f32), V((NY, ROWS, NC), f32), V((NY, ROWS, NC), bf16), V((NY - 1, ROWS, NC), bf16),
            V((NZ, 8, 128), f32), V((NZ - 1, 8, 128), f32), V((NY, NZ, 8, 128), f32),
            V((NZ, NY, ROWS, KC), bf16), V((NZ, NY, ROWS, VC), bf16), V((RK, 2 * NC), bf16), V((D, NC), f32),
            V((D, KC), bf16), V((D, VC), bf16), V((8, 128), f32), V((NT - 1, 8, 128), f32),
            V((ROWS, KC), f32), V((ROWS, VC), f32), V((ROWS, KC), f32), V((ROWS, VC), f32),
            S((2 + 3 * KCHUNKS + 2 + 6,)), S((6 + 4 + 2 * NZ,)),
            S((NY - 1,)), S((NY - 1,)), S((NZ - 1,)), S((NZ - 1,)), S((NZ - 1,)), S((NZ - 1,)), S((NY - 1,)), S((NY - 1,)),
            S((NZ - 1,)), S((NZ - 1,)), S((NY - 1,)), S((NY - 1,)),
            S((2, NY // 2, 2)), S((2, NY // 2, 2)), S((2, NZ // 2, 2)), S((2, NZ // 2, 2)),
            S((NT - 1,)), S((NT - 1,)),
        ],
        compiler_params=pltpu.CompilerParams(collective_id=0, has_side_effects=True),
    )(*args)


def solution(mesh):
    tokens, rows, cols = P(("fs", "rep"), None), P(("fs", "rep"), "tp"), P(None, "tp")
    in_specs = (tokens, rows, rows, P(), P(), rows, rows, cols, cols, cols, cols)
    out_specs = (rows, rows, cols, cols, cols, cols, rows, rows, cols, cols)
    return jax.shard_map(body, mesh=mesh, in_specs=in_specs, out_specs=out_specs, check_vma=False)
```

time: 356 us -> 74.5 us (0.21)
  the two profiles are of different devices: /device:TPU:16 before, /device:TPU:1 now
where the time goes in v1:
time: 74.5 us; the launch traced here: 73.5 us
  Pallas kernels  60.2 us (81%)
  local copies, waits for them, and re-layouts  12.6 us (17%)
    pallas_call x1, Pallas kernels, body(): pl.pallas_call(kernel, name='projected_update', out_shape=[jax.ShapeDtype...  60.2 us
    unnamed x18, local copies, waits for them, and re-layouts  12.6 us

profile of v1, /device:TPU:1, one launch (start us, length us, event | category | flops | bytes accessed | tf_op | source)
XLA Modules:
  0.0 73.5 jit_solution(450505318669475658)
XLA Ops:
  0.6 60.2 %projected_update.1 = (f32[32,128]{1,0:T(8,128)}, f32[32,256]{1,0:T(8,128)}, f32[256,128]{1,0:T(8,128)}, f32[256,128]{1,0:T(8,128)}, f32[256,256]{1,0:T(8,128)},...) custom-call(bf16[640,3072]{1,0:T(8,128)(2,1)} %x_hbm.1, ...), custom_call_target="tpu_custom_call" | custom-call | tf_op jit(solution)/shard_map/projected_update/pallas_call | solution.py:329
  60.9 0.0 copy-start.3
  60.9 0.0 copy-start.2
  60.9 0.0 copy-start.1
  60.9 1.4 %copy.31 = f32[32,128]{1,0:T(8,128)} copy(f32[32,128]{1,0:T(8,128)} %get-tuple-element.20) | data formatting | bytes 32768
  62.3 1.4 %copy.32 = f32[32,256]{1,0:T(8,128)} copy(f32[32,256]{1,0:T(8,128)} %get-tuple-element.21) | data formatting | bytes 65536
  63.7 0.0 copy-start
  63.7 1.7 %copy.33 = f32[256,128]{1,0:T(8,128)} copy(f32[256,128]{1,0:T(8,128)} %get-tuple-element.22) | data formatting | bytes 262144
  65.4 1.6 %copy.34 = f32[256,128]{1,0:T(8,128)} copy(f32[256,128]{1,0:T(8,128)} %get-tuple-element.23) | data formatting | bytes 262144
  67.0 1.7 %copy.35 = f32[256,256]{1,0:T(8,128)} copy(f32[256,256]{1,0:T(8,128)} %get-tuple-element.24) | data formatting | bytes 524288
  68.6 1.7 %copy.36 = f32[256,256]{1,0:T(8,128)} copy(f32[256,256]{1,0:T(8,128)} %get-tuple-element.25) | data formatting | bytes 524288
  70.3 0.0 copy-done.3
  70.3 0.6 copy.37
  70.9 0.0 copy-done.2
  70.9 0.6 copy.38
  71.5 0.0 copy-done.1
  71.5 0.9 %copy.39 = bf16[3072,128]{1,0:T(8,128)(2,1)} copy(bf16[3072,128]{1,0:T(8,128)(2,1)S(1)} %copy-done.1) | data formatting | bytes 1572864
  72.4 0.0 copy-done
  72.4 1.1 %copy.40 = bf16[3072,256]{1,0:T(8,128)(2,1)} copy(bf16[3072,256]{1,0:T(8,128)(2,1)S(1)} %copy-done) | data formatting | bytes 3145728
Async XLA Ops:
  60.9 9.4 %copy-start.3 = (f32[32,128]{1,0:T(8,128)S(1)}, f32[32,128]{1,0:T(8,128)}, u32[]{:S(2)}) copy-start(f32[32,128]{1,0:T(8,128)} %get-tuple-element.26) | copy-start | bytes 49156
  60.9 10.0 %copy-start.2 = (f32[32,256]{1,0:T(8,128)S(1)}, f32[32,256]{1,0:T(8,128)}, u32[]{:S(2)}) copy-start(f32[32,256]{1,0:T(8,128)} %get-tuple-element.27) | copy-start | bytes 98308
  60.9 10.6 %copy-start.1 = (bf16[3072,128]{1,0:T(8,128)(2,1)S(1)}, bf16[3072,128]{1,0:T(8,128)(2,1)}, u32[]{:S(2)}) copy-start(bf16[3072,128]{1,0:T(8,128)(2,1)} %get-tuple-element.28) | copy-start | bytes 2359300
  63.7 8.7 %copy-start = (bf16[3072,256]{1,0:T(8,128)(2,1)S(1)}, bf16[3072,256]{1,0:T(8,128)(2,1)}, u32[]{:S(2)}) copy-start(bf16[3072,256]{1,0:T(8,128)(2,1)} %get-tuple-element.29) | copy-start | bytes 4718596

commit v2 on v1

v2 whole, which is shorter than its diff:
```python
import jax
import jax.numpy as jnp
from jax import lax
from jax.experimental import pallas as pl
from jax.experimental.pallas import tpu as pltpu
from jax.sharding import PartitionSpec as P

MESH = pl.DeviceIdType.MESH
D, DK, DV, RK, RV = 3072, 1024, 2048, 256, 256
NZ, NY, NT = 12, 8, 8
TOK = 640
KC, VC = 128, 256
NC = KC + VC
ROWS = 32
KCHUNKS = 4
KSIZE = D // KCHUNKS
STEP = 768
KCH, VCH = 2, 4
HELD = 2 * D * NC + 4 * D * RK + 4 * ROWS * NC + 8 * RK * NC + 4 * RK * NC + 4096
VMEM_MAIN = 67043328 - HELD - 72 * 1024

first_decay = 0.8
second_decay = 0.9
epsilon = 1e-08
learn_rate = 0.01


def kernel(
    x_hbm, ck_hbm, cv_hbm, fk_hbm, fv_hbm, wk_hbm, wv_hbm, m1k_hbm, m2k_hbm, m1v_hbm, m2v_hbm,
    kg, vg, fk, fv, wk, wv, m1, m2, normed, shrink_out,
    xs, cs_k, cs_v, basis, part, rs1_send, rs1_recv, rs2_send, rs2_recv, ag, qt, qy,
    in_sem, r1s, r1r, r2s, r2r, a1s, a1r, a2s, a2r, k1s, k1r, v1s, v1r, krs, krr, vrs, vrr, ts, tr, us, ur,
):
    z, y, t = lax.axis_index("fs"), lax.axis_index("rep"), lax.axis_index("tp")

    def zpeer(d):
        return (lax.rem(z + d, NZ), y, t)

    def ypeer(d):
        return (z, lax.rem(y + d, NY), t)

    def tpeer(d):
        return (z, y, lax.rem(t + d, NT))

    sends = []

    def send(src, dst, ssem, rsem, peer):
        copy = pltpu.make_async_remote_copy(
            src_ref=src, dst_ref=dst, send_sem=ssem, recv_sem=rsem, device_id=peer, device_id_type=MESH
        )
        copy.start()
        sends.append(copy)
        return copy

    def arrived(ref, ssem, rsem, peer):
        pltpu.make_async_remote_copy(
            src_ref=ref, dst_ref=ref, send_sem=ssem, recv_sem=rsem, device_id=peer, device_id_type=MESH
        ).wait_recv()

    loads = {}

    def load(name, src, dst):
        copy = pltpu.make_async_copy(src, dst, in_sem.at[len(loads)])
        copy.start()
        loads[name] = copy

    load("wk", wk_hbm, wk)
    load("wv", wv_hbm, wv)
    for c in range(KCHUNKS):
        ks = pl.ds(c * KSIZE, KSIZE)
        load(f"fk{c}", fk_hbm.at[ks], fk.at[ks])
        load(f"fv{c}", fv_hbm.at[ks], fv.at[ks])
        load(f"x{c}", x_hbm.at[:, ks], xs.at[:, ks])
    load("ck", ck_hbm, cs_k)
    load("cv", cv_hbm, cs_v)
    load("m1k", m1k_hbm, m1.at[0])
    load("m2k", m2k_hbm, m2.at[0])
    for c in range(2):
        cols = pl.ds(c * 128, 128)
        load(f"m1v{c}", m1v_hbm.at[:, cols], m1.at[1 + c])
        load(f"m2v{c}", m2v_hbm.at[:, cols], m2.at[1 + c])

    barrier = pltpu.get_barrier_semaphore()
    for d in range(1, NZ):
        pl.semaphore_signal(barrier, inc=1, device_id=zpeer(d), device_id_type=MESH)
    for d in range(1, NY):
        pl.semaphore_signal(barrier, inc=1, device_id=ypeer(d), device_id_type=MESH)
    for d in range(1, NT):
        pl.semaphore_signal(barrier, inc=1, device_id=tpeer(d), device_id_type=MESH)

    loads["wk"].wait()
    loads["wv"].wait()
    kg[z, y] = wk[...].astype(jnp.bfloat16)
    vg[z, y] = wv[...].astype(jnp.bfloat16)

    def basis_chunk(c):
        ks = slice(c * KSIZE, (c + 1) * KSIZE)
        for name in ("fk", "fv", "x"):
            loads[f"{name}{c}"].wait()
        xc = xs[:, ks]
        for f, cols in ((fk, slice(0, RK)), (fv, slice(RK, RK + RV))):
            term = jnp.dot(xc, f[ks, :], preferred_element_type=jnp.float32)
            if c == 0:
                basis[:, cols] = term
            else:
                basis[:, cols] += term

    basis_chunk(0)
    pl.semaphore_wait(barrier, NZ - 1 + NY - 1 + NT - 1)
    for d in range(1, NY):
        send(vg.at[z, y], vg.at[z, y], v1s.at[d - 1], v1r.at[d - 1], ypeer(d))
    for d in range(1, NZ):
        send(kg.at[z, y], kg.at[z, y], k1s.at[d - 1], k1r.at[d - 1], zpeer(d))
    for c in range(1, KCHUNKS):
        basis_chunk(c)

    loads["ck"].wait()
    loads["cv"].wait()
    dims = (((0,), (0,)), ((), ()))
    for cols, cot, outs in (
        (slice(0, RK), cs_k, slice(0, KC)),
        (slice(RK, RK + RV), cs_v, slice(KC, NC)),
    ):
        b = basis[:, cols]
        upper = b.astype(jnp.bfloat16)
        lower = (b - upper.astype(jnp.float32)).astype(jnp.bfloat16)
        p = lax.dot_general(upper, cot[...], dims, preferred_element_type=jnp.float32)
        p += lax.dot_general(lower, cot[...], dims, preferred_element_type=jnp.float32)
        part[:, :, outs] = p.reshape(NY, ROWS, outs.stop - outs.start)
        rs1_send[:, :, outs] = p.reshape(NY, ROWS, outs.stop - outs.start).astype(jnp.bfloat16)

    for d in range(1, NY):
        peer = ypeer(d)
        send(rs1_send.at[peer[1]], rs1_recv.at[d - 1], r1s.at[d - 1], r1r.at[d - 1], peer)

    def ring(block, chunks, me, n, peer_of, ssem, rsem):
        steps = n // 2

        def owner_of(direction, hops):
            return lax.rem(me + (n - hops if direction == 0 else hops), n)

        def carries(direction, s, c):
            return s < steps or (c < chunks // 2) == (direction == 0)

        def put(direction, s, c):
            ref = block(owner_of(direction, s - 1), c)
            at = direction, s - 1, c
            send(ref, ref, ssem.at[at], rsem.at[at], peer_of(1 if direction == 0 else n - 1))

        def take(direction, s, c):
            ref = block(owner_of(direction, s), c)
            at = direction, s - 1, c
            arrived(ref, ssem.at[at], rsem.at[at], peer_of(1 if direction == 0 else n - 1))
            if s < steps and carries(direction, s + 1, c):
                put(direction, s + 1, c)

        def round_(s, chosen=range(chunks)):
            for c in chosen:
                for direction in range(2):
                    if s == 0:
                        put(direction, 1, c)
                    elif carries(direction, s, c):
                        take(direction, s, c)

        return round_

    kround = ring(lambda o, c: kg.at[pl.ds(c * (NZ // KCH), NZ // KCH), o], KCH, y, NY, ypeer, krs, krr)
    vround = ring(lambda o, c: vg.at[o, pl.ds(c * (NY // VCH), NY // VCH)], VCH, z, NZ, zpeer, vrs, vrr)

    for d in range(1, NY):
        arrived(vg.at[z, lax.rem(y + NY - d, NY)], v1s.at[d - 1], v1r.at[d - 1], ypeer(d))
    vround(0)

    total = part[y]
    for d in range(1, NY):
        arrived(rs1_recv.at[d - 1], r1s.at[d - 1], r1r.at[d - 1], ypeer(d))
        total += rs1_recv[d - 1].astype(jnp.float32)
    for i in range(NZ):
        rs2_send[i] = total[8 * (i // 3) : 8 * (i // 3) + 8, 128 * (i % 3) : 128 * (i % 3) + 128]
    for d in range(1, NZ):
        peer = zpeer(d)
        send(rs2_send.at[peer[0]], rs2_recv.at[d - 1], r2s.at[d - 1], r2r.at[d - 1], peer)

    for d in range(1, NZ):
        arrived(kg.at[lax.rem(z + NZ - d, NZ), y], k1s.at[d - 1], k1r.at[d - 1], zpeer(d))
    kround(0)
    vround(1)
    kround(1)
    vround(2)

    tile = rs2_send[z]
    for d in range(1, NZ):
        arrived(rs2_recv.at[d - 1], r2s.at[d - 1], r2r.at[d - 1], zpeer(d))
        tile += rs2_recv[d - 1]
    ag[y, z] = tile
    for d in range(1, NZ):
        send(ag.at[y, z], ag.at[y, z], a1s.at[d - 1], a1r.at[d - 1], zpeer(d))

    kround(2)
    vround(3)
    kround(3)
    vround(4)

    for d in range(1, NZ):
        arrived(ag.at[y, lax.rem(z + NZ - d, NZ)], a1s.at[d - 1], a1r.at[d - 1], zpeer(d))
    halves = pl.ds(0, NZ // 2), pl.ds(NZ // 2, NZ // 2)

    def far(hops):
        return lax.rem(y + NY + hops, NY)

    def ag_send(slot, ref, hops):
        send(ref, ref, a2s.at[slot], a2r.at[slot], ypeer(NY + hops))

    def ag_arrived(slot, ref):
        arrived(ref, a2s.at[slot], a2r.at[slot], ypeer(1))

    for slot, hops in ((2, 2), (3, -2), (0, 1), (1, -1)):
        ag_send(slot, ag.at[y], hops)

    def normed_of(proj, first, second):
        first_new = first_decay * first + (1.0 - first_decay) * proj
        second_new = second_decay * second + (1.0 - second_decay) * proj * proj
        return first_new, second_new, first_new / (jnp.sqrt(second_new) + epsilon)

    for name in ("m1k", "m2k", "m1v0", "m2v0", "m1v1", "m2v1"):
        loads[name].wait()
    squares = jnp.zeros((8, 128), jnp.float32)
    for i in range(NZ):
        at = pl.ds(pl.multiple_of(ROWS * y + 8 * (i // 3), 8), 8)
        n = normed_of(ag[y, i], m1[i % 3, at], m2[i % 3, at])[2]
        squares += n * n
    qt[t] = squares
    for d in range(1, NT):
        send(qt.at[t], qt.at[t], ts.at[d - 1], tr.at[d - 1], tpeer(d))

    kround(4)
    vround(5)

    for slot, hops in ((2, 1), (3, -1)):
        owner = far(-2 * hops)
        ag_arrived(slot, ag.at[owner])
        ag_send(slot + 2, ag.at[owner], hops)
        half = ag.at[owner, halves[slot - 2]]
        ag_send(slot + 4, half, 2 * hops)

    for d in range(1, NT):
        arrived(qt.at[lax.rem(t + NT - d, NT)], ts.at[d - 1], tr.at[d - 1], tpeer(d))
    squares = qt[0]
    for i in range(1, NT):
        squares += qt[i]
    qy[y] = squares
    for d in range(1, NY):
        send(qy.at[y], qy.at[y], us.at[d - 1], ur.at[d - 1], ypeer(d))

    vround(6)

    for slot, hops in ((0, -1), (1, 1), (4, -3), (5, 3)):
        ag_arrived(slot, ag.at[far(hops)])
    ag_arrived(6, ag.at[far(4), halves[0]])
    ag_arrived(7, ag.at[far(4), halves[1]])

    for g in range(3):
        proj = jnp.concatenate([ag[b, 3 * i + g] for b in range(NY) for i in range(4)], axis=0)
        first_new, second_new, n = normed_of(proj, m1[g], m2[g])
        m1[g] = first_new
        m2[g] = second_new
        upper = n.astype(jnp.bfloat16)
        lower = (n - upper.astype(jnp.float32)).astype(jnp.bfloat16)
        at = (0, 256, 384)[g]
        normed[:, at : at + 128] = upper
        at = (128, 512, 640)[g]
        normed[:, at : at + 128] = lower

    for d in range(1, NY):
        arrived(qy.at[lax.rem(y + NY - d, NY)], us.at[d - 1], ur.at[d - 1], ypeer(d))
    squares = qy[0]
    for i in range(1, NY):
        squares += qy[i]
    whole = jnp.sum(jnp.sum(squares, axis=0, keepdims=True), axis=1, keepdims=True)
    entries = float(RK * DK + RV * DV)
    shrink_out[...] = jnp.broadcast_to(jnp.sqrt(entries / (entries + whole)), (8, 128))

    for copy in sends:
        copy.wait_send()


def finish(
    kg, vg, fk, fv, wk, wv, m1, m2, normed, shrink_in,
    wkn_hbm, wvn_hbm, m1kn_hbm, m2kn_hbm, m1vn_hbm, m2vn_hbm, sk_hbm, sv_hbm, kcopy_hbm, vcopy_hbm,
    kout, vout, ok, ov, osk, osv, out_sem,
):
    z, y = lax.axis_index("fs"), lax.axis_index("rep")
    outs = []

    def store(src, dst):
        copy = pltpu.make_async_copy(src, dst, out_sem.at[len(outs)])
        copy.start()
        outs.append(copy)

    store(m1.at[0], m1kn_hbm)
    store(m2.at[0], m2kn_hbm)
    for c in range(2):
        cols = pl.ds(c * 128, 128)
        store(m1.at[1 + c], m1vn_hbm.at[:, cols])
        store(m2.at[1 + c], m2vn_hbm.at[:, cols])

    shrink = shrink_in[0:1, 0:1]

    def steps_of(rows):
        wide = jnp.dot(fk[rows, :], normed[:, 0:256], preferred_element_type=jnp.float32)
        tall = jnp.dot(fv[rows, :], normed[:, 256:512], preferred_element_type=jnp.float32)
        tall += jnp.dot(fv[rows, :], normed[:, 512:768], preferred_element_type=jnp.float32)
        return shrink * (wide[:, :KC] + wide[:, KC:]), shrink * tall

    blocks = STEP // 256
    for b in range(D // STEP):
        rows = slice(b * STEP, b * STEP + STEP)
        key_step, value_step = steps_of(rows)
        kw = kg[blocks * b : blocks * b + blocks].reshape(STEP, KC).astype(jnp.float32)
        kout[rows, :] = (kw - learn_rate * key_step).astype(jnp.bfloat16)
        vw = vg[blocks * b : blocks * b + blocks].reshape(STEP, VC).astype(jnp.float32)
        vout[rows, :] = (vw - learn_rate * value_step).astype(jnp.bfloat16)
        store(kout.at[pl.ds(b * STEP, STEP)], kcopy_hbm.at[pl.ds(b * STEP, STEP)])
        store(vout.at[pl.ds(b * STEP, STEP)], vcopy_hbm.at[pl.ds(b * STEP, STEP)])

    key_step, value_step = steps_of(pl.ds(pl.multiple_of((z * NY + y) * ROWS, ROWS), ROWS))
    osk[...] = key_step
    osv[...] = value_step
    ok[...] = wk[...] - learn_rate * key_step
    ov[...] = wv[...] - learn_rate * value_step
    store(osk, sk_hbm)
    store(osv, sv_hbm)
    store(ok, wkn_hbm)
    store(ov, wvn_hbm)
    for copy in outs:
        copy.wait()


def body(*args):
    f32, bf16 = jnp.float32, jnp.bfloat16
    V, S = pltpu.VMEM, pltpu.SemaphoreType.DMA
    outs = [
        ((ROWS, KC), f32), ((ROWS, VC), f32), ((RK, KC), f32), ((RK, KC), f32), ((RV, VC), f32), ((RV, VC), f32),
        ((ROWS, KC), f32), ((ROWS, VC), f32), ((D, KC), bf16), ((D, VC), bf16),
    ]
    held = [
        V((NZ, NY, ROWS, KC), bf16), V((NZ, NY, ROWS, VC), bf16), V((D, RK), bf16), V((D, RV), bf16),
        V((ROWS, KC), f32), V((ROWS, VC), f32), V((3, RK, 128), f32), V((3, RK, 128), f32), V((RK, 2 * NC), bf16),
        V((8, 128), f32),
    ]
    held_specs = [pl.BlockSpec(memory_space=V)] * len(held)
    middle = pl.pallas_call(
        kernel,
        name="projected_update",
        out_shape=held,
        in_specs=[pl.BlockSpec(memory_space=pltpu.HBM)] * 11,
        out_specs=held_specs,
        scratch_shapes=[
            V((TOK, D), bf16), V((TOK, KC), bf16), V((TOK, VC), bf16),
            V((TOK, RK + RV), f32), V((NY, ROWS, NC), f32), V((NY, ROWS, NC), bf16), V((NY - 1, ROWS, NC), bf16),
            V((NZ, 8, 128), f32), V((NZ - 1, 8, 128), f32), V((NY, NZ, 8, 128), f32),
            V((NT, 8, 128), f32), V((NY, 8, 128), f32),
            S((2 + 3 * KCHUNKS + 2 + 6,)),
            S((NY - 1,)), S((NY - 1,)), S((NZ - 1,)), S((NZ - 1,)), S((NZ - 1,)), S((NZ - 1,)), S((8,)), S((8,)),
            S((NZ - 1,)), S((NZ - 1,)), S((NY - 1,)), S((NY - 1,)),
            S((2, NY // 2, KCH)), S((2, NY // 2, KCH)), S((2, NZ // 2, VCH)), S((2, NZ // 2, VCH)),
            S((NT - 1,)), S((NT - 1,)), S((NY - 1,)), S((NY - 1,)),
        ],
        compiler_params=pltpu.CompilerParams(collective_id=0, has_side_effects=True, vmem_limit_bytes=VMEM_MAIN),
    )(*args)
    return pl.pallas_call(
        finish,
        name="finish",
        out_shape=[jax.ShapeDtypeStruct(s, dt) for s, dt in outs],
        in_specs=held_specs,
        out_specs=[pl.BlockSpec(memory_space=pltpu.HBM)] * len(outs),
        scratch_shapes=[
            V((D, KC), bf16), V((D, VC), bf16),
            V((ROWS, KC), f32), V((ROWS, VC), f32), V((ROWS, KC), f32), V((ROWS, VC), f32),
            S((10 + 2 * (D // STEP),)),
        ],
        compiler_params=pltpu.CompilerParams(vmem_limit_bytes=16 << 20),
    )(*middle)


def solution(mesh):
    tokens, rows, cols = P(("fs", "rep"), None), P(("fs", "rep"), "tp"), P(None, "tp")
    in_specs = (tokens, rows, rows, P(), P(), rows, rows, cols, cols, cols, cols)
    out_specs = (rows, rows, cols, cols, cols, cols, rows, rows, cols, cols)
    return jax.shard_map(body, mesh=mesh, in_specs=in_specs, out_specs=out_specs, check_vma=False)
```

time: 74.5 us -> 59.6 us (0.80)
  local copies, waits for them, and re-layouts: 12.6 us -> 0 us
  Pallas kernels: 60.2 us -> 58 us
    unnamed x18 -> x0, local copies, waits for them, and re-layouts: 12.6 us -> none
    pallas_call x1 -> x2, Pallas kernels: 60.2 us -> 58 us  [the longest x1 55.4 us: body(): pl.pallas_call(kernel, name='projected_update', out_shape=held, in_specs=...]
where the time goes in v2:
time: 59.6 us; the launch traced here: 58.7 us
  Pallas kernels  58 us (97%)
  between operations  0.65 us (1%)
    pallas_call x1, Pallas kernels, body(): pl.pallas_call(kernel, name='projected_update', out_shape=held, in_specs=...  55.4 us
    pallas_call x1, Pallas kernels, body(): pl.pallas_call(finish, name='finish', out_shape=[jax.ShapeDtypeStruct(s,...  2.57 us

profile of v2, /device:TPU:1, one launch (start us, length us, event | category | flops | bytes accessed | tf_op | source)
XLA Modules:
  0.0 58.7 jit_solution(5034055349580010967)
XLA Ops:
  0.6 55.4 %projected_update.1 = (bf16[12,8,32,128]{3,2,1,0:T(8,128)(2,1)S(1)}, bf16[12,8,32,256]{3,2,1,0:T(8,128)(2,1)S(1)}, bf16[3072,256]{1,0:T(8,128)(2,1)S(1)}, bf16[3...) custom-call(bf16[640,3072]{1,0:T(8,128)(2,1)} %x_hbm.1, ...), custom_call_target="tpu_custom_call" | custom-call | tf_op jit(solution)/shard_map/projected_update/pallas_call | solution.py:352
  56.1 2.6 %finish.1 = (f32[32,128]{1,0:T(8,128)}, f32[32,256]{1,0:T(8,128)}, f32[256,128]{1,0:T(8,128)}, f32[256,128]{1,0:T(8,128)}, f32[256,256]{1,0:T(8,128)}, /*index=5...) custom-call(bf16[12,8,32,128]{3,2,1,0:T(8,128)(2,1)S(1)} %get-tuple-, ...), custom_call_target="tpu_custom_call" | custom-call | tf_op jit(solution)/shard_map/finish/pallas_call | solution.py:371

commit v3 on v2

v3 whole, which is shorter than its diff:
```python
import jax
import jax.numpy as jnp
from jax import lax
from jax.experimental import pallas as pl
from jax.experimental.pallas import tpu as pltpu
from jax.sharding import PartitionSpec as P

MESH = pl.DeviceIdType.MESH
D, DK, DV, RK, RV = 3072, 1024, 2048, 256, 256
NZ, NY, NT = 12, 8, 8
TOK = 640
KC, VC = 128, 256
NC = KC + VC
ROWS = 32
KAT = (0, 512, 1536, 2560, 3072)
KCHUNKS = len(KAT) - 1
FAR_Y = (4, 3, 5, 2, 6, 1, 7)
NEAR_FIRST_Y = (1, 7, 6, 2, 5, 3, 4)
FAR_Z = (6, 5, 7, 4, 8, 3, 9, 2, 10, 1, 11)
VALUE, VALUE_FAR, KEY, RS_REP, RS_REP_FAR, RS_FS, AG_FS, AG_FS_FAR, AG_REP, SQ_REP, SQ_TP, KEY_RING, VALUE_RING = range(13)
GROUPS = 13
NEAR, NEAR_Y = 2, 1
STEP = 512
KCH, VCH = 2, 4
HELD = 2 * D * NC + 4 * D * RK + 4 * ROWS * NC + 8 * RK * NC + 4 * RK * NC + 4096
VMEM_MAIN = 67043328 - HELD - 72 * 1024

first_decay = 0.8
second_decay = 0.9
epsilon = 1e-08
learn_rate = 0.01


def kernel(
    x_hbm, ck_hbm, cv_hbm, fk_hbm, fv_hbm, wk_hbm, wv_hbm, m1k_hbm, m2k_hbm, m1v_hbm, m2v_hbm,
    kg, vg, fk, fv, wk, wv, mm, normed, shrink_out,
    xs, cs_k, cs_v, basis, part, rs1_send, rs1_recv, rs2_send, rs2_recv, ag, qt, qy,
    in_sem, out_sems, in_sems, a2r, krr, vrr,
):
    z, y, t = lax.axis_index("fs"), lax.axis_index("rep"), lax.axis_index("tp")

    def zpeer(d):
        return (lax.rem(z + d, NZ), y, t)

    def ypeer(d):
        return (z, lax.rem(y + d, NY), t)

    def tpeer(d):
        return (z, y, lax.rem(t + d, NT))

    def copy_of(src, dst, ssem, rsem, peer):
        return pltpu.make_async_remote_copy(
            src_ref=src, dst_ref=dst, send_sem=ssem, recv_sem=rsem, device_id=peer, device_id_type=MESH
        )

    def send(src, dst, group, peer, rsem=None):
        copy_of(src, dst, out_sems.at[group], in_sems.at[group] if rsem is None else rsem, peer).start()

    def arrived(ref, group=None, rsem=None):
        copy_of(ref, ref, out_sems.at[0], in_sems.at[group] if rsem is None else rsem, zpeer(1)).wait_recv()

    def sent(ref, group):
        copy_of(ref, ref, out_sems.at[group], in_sems.at[group], zpeer(1)).wait_send()

    loads = {}

    def load(name, src, dst):
        copy = pltpu.make_async_copy(src, dst, in_sem.at[len(loads)])
        copy.start()
        loads[name] = copy

    def load_chunk(c):
        ks = pl.ds(KAT[c], KAT[c + 1] - KAT[c])
        load(f"fk{c}", fk_hbm.at[ks], fk.at[ks])
        load(f"fv{c}", fv_hbm.at[ks], fv.at[ks])
        load(f"x{c}", x_hbm.at[:, ks], xs.at[:, ks])

    load_chunk(0)
    load("wk", wk_hbm, wk)
    load("wv", wv_hbm, wv)
    for c in range(1, KCHUNKS):
        load_chunk(c)
    load("ck", ck_hbm, cs_k)
    load("cv", cv_hbm, cs_v)
    moments_sem = in_sem.at[len(loads)]
    for src, dst in (
        (m1k_hbm, 0), (m1v_hbm.at[:, pl.ds(0, 128)], 1), (m1v_hbm.at[:, pl.ds(128, 128)], 2),
        (m2k_hbm, 3), (m2v_hbm.at[:, pl.ds(0, 128)], 4), (m2v_hbm.at[:, pl.ds(128, 128)], 5),
    ):
        pltpu.make_async_copy(src, mm.at[dst], moments_sem).start()

    barrier = pltpu.get_barrier_semaphore()
    for d in range(1, NZ):
        pl.semaphore_signal(barrier, inc=1, device_id=zpeer(d), device_id_type=MESH)
    for d in range(1, NY):
        pl.semaphore_signal(barrier, inc=1, device_id=ypeer(d), device_id_type=MESH)
    for d in range(1, NT):
        pl.semaphore_signal(barrier, inc=1, device_id=tpeer(d), device_id_type=MESH)

    def basis_chunk(c):
        ks = slice(KAT[c], KAT[c + 1])
        for name in ("fk", "fv", "x"):
            loads[f"{name}{c}"].wait()
        xc = xs[:, ks]
        for f, cols in ((fk, slice(0, RK)), (fv, slice(RK, RK + RV))):
            term = jnp.dot(xc, f[ks, :], preferred_element_type=jnp.float32)
            if c == 0:
                basis[:, cols] = term
            else:
                basis[:, cols] += term

    basis_chunk(0)
    loads["wk"].wait()
    loads["wv"].wait()
    kg[z, y] = wk[...].astype(jnp.bfloat16)
    vg[z, NEAR_Y] = wv[...].astype(jnp.bfloat16)
    pl.semaphore_wait(barrier, NZ - 1 + NY - 1 + NT - 1)
    for d in NEAR_FIRST_Y:
        slot = (NEAR_Y - d) % NY
        send(vg.at[z, NEAR_Y], vg.at[z, slot], VALUE if slot < NY // 2 else VALUE_FAR, ypeer(d))
    for d in FAR_Z:
        send(kg.at[z, y], kg.at[z, y], KEY, zpeer(d))
    for c in range(1, KCHUNKS):
        basis_chunk(c)

    slots = [lax.rem(i - z + NZ + NEAR, NZ) for i in range(NZ)]
    near, beyond = pl.ds(0, NZ // 2), pl.ds(NZ // 2, NZ // 2)

    loads["ck"].wait()
    loads["cv"].wait()
    dims = (((0,), (0,)), ((), ()))
    for cols, cot, outs in (
        (slice(0, RK), cs_k, slice(0, KC)),
        (slice(RK, RK + RV), cs_v, slice(KC, NC)),
    ):
        b = basis[:, cols]
        upper = b.astype(jnp.bfloat16)
        lower = (b - upper.astype(jnp.float32)).astype(jnp.bfloat16)
        p = lax.dot_general(upper, cot[...], dims, preferred_element_type=jnp.float32)
        p += lax.dot_general(lower, cot[...], dims, preferred_element_type=jnp.float32)
        for b in range(NY):
            for i in range(outs.start // 128, NZ):
                if outs.start <= 128 * (i % 3) < outs.stop:
                    at = ROWS * b + 8 * (i // 3)
                    lanes = 128 * (i % 3) - outs.start
                    piece = p[at : at + 8, lanes : lanes + 128]
                    part[b, slots[i]] = piece
                    rs1_send[b, slots[i]] = piece.astype(jnp.bfloat16)

    for tiles, group in ((beyond, RS_REP_FAR), (near, RS_REP)):
        for d in FAR_Y:
            peer = ypeer(d)
            send(rs1_send.at[peer[1], tiles], rs1_recv.at[d - 1, tiles], group, peer)

    def ring(block, chunks, me, n, peer_of, group, rsem):
        steps = n // 2

        def owner_of(direction, hops):
            return lax.rem(me + (n - hops if direction == 0 else hops), n)

        def carries(direction, s, c):
            return s < steps or (c < chunks // 2) == (direction == 0)

        def put(direction, s, c):
            ref = block(owner_of(direction, s - 1), c)
            send(ref, ref, group, peer_of(1 if direction == 0 else n - 1), rsem.at[direction, s - 1, c])

        def take(direction, s, c):
            arrived(block(owner_of(direction, s), c), rsem=rsem.at[direction, s - 1, c])
            if s < steps and carries(direction, s + 1, c):
                put(direction, s + 1, c)

        def round_(s, chosen=range(chunks)):
            for c in chosen:
                for direction in range(2):
                    if s == 0:
                        put(direction, 1, c)
                    elif carries(direction, s, c):
                        take(direction, s, c)

        return round_

    kround = ring(lambda o, c: kg.at[pl.ds(c * (NZ // KCH), NZ // KCH), o], KCH, y, NY, ypeer, KEY_RING, krr)
    vround = ring(lambda o, c: vg.at[o, pl.ds(c * (NY // VCH), NY // VCH)], VCH, z, NZ, zpeer, VALUE_RING, vrr)

    lower, upper = range(VCH // 2), range(VCH // 2, VCH)

    arrived(vg.at[z, pl.ds(0, NY // 2 - 1)], VALUE)
    vround(0, lower)
    arrived(vg.at[z, pl.ds(NY // 2, NY // 2)], VALUE_FAR)
    vround(0, upper)
    vround(1, lower)

    for tiles, group, order in (
        (beyond, RS_REP_FAR, (6, 5, 7, 4, 8, 9)), (near, RS_REP, (3, 2, 10, 1, 11, 0)),
    ):
        arrived(rs1_recv.at[:, tiles], group)
        for d in order:
            slot = (d + NEAR) % NZ
            total = part[y, slot]
            for i in range(NY - 1):
                total += rs1_recv[i, slot].astype(jnp.float32)
            rs2_send[slot] = total
        for d in order:
            if d:
                send(rs2_send.at[(d + NEAR) % NZ], rs2_recv.at[d - 1], RS_FS, zpeer(d))

    arrived(kg.at[pl.ds(0, NZ - 1), y], KEY)
    kround(0)
    vround(1, upper)
    vround(2, lower)
    kround(1)
    vround(2, upper)
    vround(3, lower)

    tile = rs2_send[NEAR]
    arrived(rs2_recv, RS_FS)
    for d in range(1, NZ):
        tile += rs2_recv[d - 1]
    ag[y, NEAR] = tile
    for d in FAR_Z:
        slot = (NEAR - d) % NZ
        send(ag.at[y, NEAR], ag.at[y, slot], AG_FS if slot < NZ // 2 else AG_FS_FAR, zpeer(d))

    kround(2)
    vround(3, upper)
    vround(4, lower)
    kround(3)

    def ag_send(ref, hops, rsem=None):
        send(ref, ref, AG_REP, ypeer(NY + hops), rsem)

    def ag_own(p, tiles):
        for hops, which in ((2, 0), (-2, 1)):
            ag_send(ag.at[y, tiles], hops, a2r.at[which, p])
        for hops in (1, -1):
            ag_send(ag.at[y, tiles], hops)

    def ag_pass(p, tiles):
        for hops, which in ((1, 0), (-1, 1)):
            ref = ag.at[lax.rem(y + NY - 2 * hops, NY), tiles]
            arrived(ref, rsem=a2r.at[which, p])
            ag_send(ref, hops)
            if which == p:
                ag_send(ref, 2 * hops)

    arrived(ag.at[y, pl.ds(0, NZ // 2 - 1)], AG_FS)
    ag_own(0, near)

    vround(4, upper)

    arrived(ag.at[y, beyond], AG_FS_FAR)

    def normed_of(proj, first, second):
        first_new = first_decay * first + (1.0 - first_decay) * proj
        second_new = second_decay * second + (1.0 - second_decay) * proj * proj
        return first_new, second_new, first_new / (jnp.sqrt(second_new) + epsilon)

    pltpu.make_async_copy(mm, mm, moments_sem).wait()
    squares = jnp.zeros((8, 128), jnp.float32)
    for i in range(NZ):
        at = pl.ds(pl.multiple_of(ROWS * y + 8 * (i // 3), 8), 8)
        n = normed_of(ag[y, slots[i]], mm[i % 3, at], mm[3 + i % 3, at])[2]
        squares += n * n
    qy[y] = squares
    for d in FAR_Y:
        send(qy.at[y], qy.at[y], SQ_REP, ypeer(d))
    ag_own(1, beyond)

    vround(5, lower)

    ag_pass(0, near)

    vround(5, upper)

    arrived(qy.at[pl.ds(0, NY - 1)], SQ_REP)
    squares = qy[0]
    for i in range(1, NY):
        squares += qy[i]
    qt[t] = squares
    for d in range(1, NT):
        send(qt.at[t], qt.at[t], SQ_TP, tpeer(d))

    ag_pass(1, beyond)

    kround(4)
    vround(6)

    arrived(ag.at[pl.ds(0, NY - 3)], AG_REP)

    for g in range(3):
        proj = jnp.concatenate([ag[b, slots[3 * i + g]] for b in range(NY) for i in range(4)], axis=0)
        first_new, second_new, n = normed_of(proj, mm[g], mm[3 + g])
        mm[g] = first_new
        mm[3 + g] = second_new
        upper = n.astype(jnp.bfloat16)
        lower = (n - upper.astype(jnp.float32)).astype(jnp.bfloat16)
        normed[:, 128 * g : 128 * g + 128] = upper
        normed[:, NC + 128 * g : NC + 128 * g + 128] = lower

    arrived(qt.at[pl.ds(0, NT - 1)], SQ_TP)
    squares = qt[0]
    for i in range(1, NT):
        squares += qt[i]
    whole = jnp.sum(jnp.sum(squares, axis=0, keepdims=True), axis=1, keepdims=True)
    entries = float(RK * DK + RV * DV)
    shrink_out[...] = jnp.broadcast_to(jnp.sqrt(entries / (entries + whole)), (8, 128))

    sent(vg.at[z, pl.ds(0, NY // 2 - 1)], VALUE)
    sent(vg.at[z, pl.ds(NY // 2, NY // 2)], VALUE_FAR)
    sent(kg.at[pl.ds(0, NZ - 1), y], KEY)
    sent(rs1_recv.at[:, near], RS_REP)
    sent(rs1_recv.at[:, beyond], RS_REP_FAR)
    sent(rs2_recv, RS_FS)
    sent(ag.at[y, pl.ds(0, NZ // 2 - 1)], AG_FS)
    sent(ag.at[y, beyond], AG_FS_FAR)
    sent(ag.at[pl.ds(0, NY - 1)], AG_REP)
    sent(qy.at[pl.ds(0, NY - 1)], SQ_REP)
    sent(qt.at[pl.ds(0, NT - 1)], SQ_TP)
    sent(kg.at[:, pl.ds(0, NY - 1)], KEY_RING)
    sent(vg.at[pl.ds(0, NZ - 1)], VALUE_RING)


def finish(
    kg, vg, fk, fv, wk, wv, mm, normed, shrink_in,
    wkn_hbm, wvn_hbm, m1kn_hbm, m2kn_hbm, m1vn_hbm, m2vn_hbm, sk_hbm, sv_hbm, kcopy_hbm, vcopy_hbm,
    kout, vout, ok, ov, osk, osv, out_sem,
):
    z, y = lax.axis_index("fs"), lax.axis_index("rep")
    outs = []

    def store(src, dst):
        copy = pltpu.make_async_copy(src, dst, out_sem.at[len(outs)])
        copy.start()
        outs.append(copy)

    for src, dst in (
        (0, m1kn_hbm), (1, m1vn_hbm.at[:, pl.ds(0, 128)]), (2, m1vn_hbm.at[:, pl.ds(128, 128)]),
        (3, m2kn_hbm), (4, m2vn_hbm.at[:, pl.ds(0, 128)]), (5, m2vn_hbm.at[:, pl.ds(128, 128)]),
    ):
        store(mm.at[src], dst)

    shrink = shrink_in[0:1, 0:1]

    def steps_of(rows, parts):
        key_step = value_step = 0.0
        for at in parts:
            key_step += jnp.dot(fk[rows, :], normed[:, at : at + KC], preferred_element_type=jnp.float32)
            value_step += jnp.dot(fv[rows, :], normed[:, at + KC : at + NC], preferred_element_type=jnp.float32)
        return shrink * key_step, shrink * value_step

    blocks = STEP // 256
    for b in range(D // STEP):
        rows = slice(b * STEP, b * STEP + STEP)
        key_step, value_step = steps_of(rows, (0,))
        kw = kg[blocks * b : blocks * b + blocks].reshape(STEP, KC).astype(jnp.float32)
        kout[rows, :] = (kw - learn_rate * key_step).astype(jnp.bfloat16)
        vw = jnp.concatenate(
            [vg[blocks * b + i, lax.rem(j - y + NY + NEAR_Y, NY)] for i in range(blocks) for j in range(NY)], axis=0
        ).astype(jnp.float32)
        vout[rows, :] = (vw - learn_rate * value_step).astype(jnp.bfloat16)
        store(kout.at[pl.ds(b * STEP, STEP)], kcopy_hbm.at[pl.ds(b * STEP, STEP)])
        store(vout.at[pl.ds(b * STEP, STEP)], vcopy_hbm.at[pl.ds(b * STEP, STEP)])

    key_step, value_step = steps_of(pl.ds(pl.multiple_of((z * NY + y) * ROWS, ROWS), ROWS), (0, NC))
    osk[...] = key_step
    osv[...] = value_step
    ok[...] = wk[...] - learn_rate * key_step
    ov[...] = wv[...] - learn_rate * value_step
    store(osk, sk_hbm)
    store(osv, sv_hbm)
    store(ok, wkn_hbm)
    store(ov, wvn_hbm)
    for copy in outs:
        copy.wait()


def body(*args):
    f32, bf16 = jnp.float32, jnp.bfloat16
    V, S = pltpu.VMEM, pltpu.SemaphoreType.DMA
    outs = [
        ((ROWS, KC), f32), ((ROWS, VC), f32), ((RK, KC), f32), ((RK, KC), f32), ((RV, VC), f32), ((RV, VC), f32),
        ((ROWS, KC), f32), ((ROWS, VC), f32), ((D, KC), bf16), ((D, VC), bf16),
    ]
    held = [
        V((NZ, NY, ROWS, KC), bf16), V((NZ, NY, ROWS, VC), bf16), V((D, RK), bf16), V((D, RV), bf16),
        V((ROWS, KC), f32), V((ROWS, VC), f32), V((6, RK, 128), f32), V((RK, 2 * NC), bf16), V((8, 128), f32),
    ]
    held_specs = [pl.BlockSpec(memory_space=V)] * len(held)
    middle = pl.pallas_call(
        kernel,
        name="projected_update",
        out_shape=held,
        in_specs=[pl.BlockSpec(memory_space=pltpu.HBM)] * 11,
        out_specs=held_specs,
        scratch_shapes=[
            V((TOK, D), bf16), V((TOK, KC), bf16), V((TOK, VC), bf16),
            V((TOK, RK + RV), f32), V((NY, NZ, 8, 128), f32), V((NY, NZ, 8, 128), bf16), V((NY - 1, NZ, 8, 128), bf16),
            V((NZ, 8, 128), f32), V((NZ - 1, 8, 128), f32), V((NY, NZ, 8, 128), f32),
            V((NT, 8, 128), f32), V((NY, 8, 128), f32),
            S((2 + 3 * KCHUNKS + 2 + 1,)), S((GROUPS,)), S((GROUPS,)), S((2, 2)),
            S((2, NY // 2, KCH)), S((2, NZ // 2, VCH)),
        ],
        compiler_params=pltpu.CompilerParams(collective_id=0, has_side_effects=True, vmem_limit_bytes=VMEM_MAIN),
    )(*args)
    return pl.pallas_call(
        finish,
        name="finish",
        out_shape=[jax.ShapeDtypeStruct(s, dt) for s, dt in outs],
        in_specs=held_specs,
        out_specs=[pl.BlockSpec(memory_space=pltpu.HBM)] * len(outs),
        scratch_shapes=[
            V((D, KC), bf16), V((D, VC), bf16),
            V((ROWS, KC), f32), V((ROWS, VC), f32), V((ROWS, KC), f32), V((ROWS, VC), f32),
            S((10 + 2 * (D // STEP),)),
        ],
        compiler_params=pltpu.CompilerParams(vmem_limit_bytes=16 << 20),
    )(*middle)


def solution(mesh):
    tokens, rows, cols = P(("fs", "rep"), None), P(("fs", "rep"), "tp"), P(None, "tp")
    in_specs = (tokens, rows, rows, P(), P(), rows, rows, cols, cols, cols, cols)
    out_specs = (rows, rows, cols, cols, cols, cols, rows, rows, cols, cols)
    return jax.shard_map(body, mesh=mesh, in_specs=in_specs, out_specs=out_specs, check_vma=False)
```

time: 59.6 us -> 55.4 us (0.930); the launches traced: 58.7 us -> 55.3 us
  Pallas kernels: 58 us -> 54.7 us
    pallas_call x1, Pallas kernels: 55.4 us -> 52.6 us  [body(): pl.pallas_call(kernel, name='projected_update', out_shape=held, in_specs=...]
where the time goes in v3:
time: 55.4 us; the launch traced here: 55.3 us
  Pallas kernels  54.7 us (99%)
  between operations  0.65 us (1%)
    pallas_call x1, Pallas kernels, body(): pl.pallas_call(kernel, name='projected_update', out_shape=held, in_specs=...  52.6 us
    pallas_call x1, Pallas kernels, body(): pl.pallas_call(finish, name='finish', out_shape=[jax.ShapeDtypeStruct(s,...  2 us

profile of v3, /device:TPU:1, one launch (start us, length us, event | category | flops | bytes accessed | tf_op | source)
XLA Modules:
  0.0 55.3 jit_solution(16472577075288353280)
XLA Ops:
  0.6 52.6 %projected_update.1 = (bf16[12,8,32,128]{3,2,1,0:T(8,128)(2,1)S(1)}, bf16[12,8,32,256]{3,2,1,0:T(8,128)(2,1)S(1)}, bf16[3072,256]{1,0:T(8,128)(2,1)S(1)}, bf16[3...) custom-call(bf16[640,3072]{1,0:T(8,128)(2,1)} %x_hbm.1, ...), custom_call_target="tpu_custom_call" | custom-call | tf_op jit(solution)/shard_map/projected_update/pallas_call | solution.py:390
  53.3 2.0 %finish.1 = (f32[32,128]{1,0:T(8,128)}, f32[32,256]{1,0:T(8,128)}, f32[256,128]{1,0:T(8,128)}, f32[256,128]{1,0:T(8,128)}, f32[256,256]{1,0:T(8,128)}, /*index=5...) custom-call(bf16[12,8,32,128]{3,2,1,0:T(8,128)(2,1)S(1)} %get-tuple-, ...), custom_call_target="tpu_custom_call" | custom-call | tf_op jit(solution)/shard_map/finish/pallas_call | solution.py:406

commit v4 on v3

v4 whole, which is shorter than its diff:
```python
import jax
import jax.numpy as jnp
from jax import lax
from jax.experimental import pallas as pl
from jax.experimental.pallas import tpu as pltpu
from jax.sharding import PartitionSpec as P

MESH = pl.DeviceIdType.MESH
D, DK, DV, RK, RV = 3072, 1024, 2048, 256, 256
NZ, NY, NT, NX = 12, 8, 8, 4
TOK = 640
KC, VC = 128, 256
NC = KC + VC
ROWS = 32
KAT = (0, 512, 1536, 2560, 3072)
KCHUNKS = len(KAT) - 1
FAR_Y = (4, 3, 5, 2, 6, 1, 7)
NEAR_FIRST_Y = (1, 7, 6, 2, 5, 3, 4)
FAR_Z = (6, 5, 7, 4, 8, 3, 9, 2, 10, 1, 11)
VALUE, VALUE_FAR, KEY, VALUE_TWIN, KEY_TWIN, MOMENTS_TWIN, AG_TWIN, SQ_TWIN = range(8)
RS_REP, RS_REP_FAR = 8, 10
RS_FS, AG_FS, AG_FS_FAR, AG_REP, SQ_REP, SQ_TP, KEY_RING, VALUE_RING = range(12, 20)
VALUE_HOME, KEY_HOME, VALUE_RING_HOME, KEY_RING_HOME = range(20, 24)
GROUPS = 24
NEAR, NEAR_Y = 2, 1
STEP = 512
KCH, VCH = 2, 4
HELD = 4 * D * NC + 4 * D * RK + 4 * ROWS * NC + 8 * RK * NC + 4 * RK * NC + 4096
VMEM_MAIN = 67043328 - HELD - 72 * 1024

first_decay = 0.8
second_decay = 0.9
epsilon = 1e-08
learn_rate = 0.01


def kernel(
    x_hbm, ck_hbm, cv_hbm, fk_hbm, fv_hbm, wk_hbm, wv_hbm, m1k_hbm, m2k_hbm, m1v_hbm, m2v_hbm,
    kg, vg, fk, fv, wk, wv, mm, normed, shrink_out,
    xs, cs_k, cs_v, basis, part, rs1_send, rs1_recv, rs2_send, rs2_recv, ag, qt, qy, total_sq, twin_mm,
    in_sem, out_sems, in_sems, a2r, krr, vrr,
):
    z, y, t = lax.axis_index("fs"), lax.axis_index("rep"), lax.axis_index("tp")

    core = lax.rem(t, 2)
    first, second = t - core, t - core + 1
    mover, adder = core == 0, core == 1
    other = (z, y, t + 1 - 2 * core)
    x = t // 2

    def zpeer(d, tp):
        return (lax.rem(z + d, NZ), y, tp)

    def ypeer(d, tp):
        return (z, lax.rem(y + d, NY), tp)

    def copy_of(src, dst, ssem, rsem, peer):
        return pltpu.make_async_remote_copy(
            src_ref=src, dst_ref=dst, send_sem=ssem, recv_sem=rsem, device_id=peer, device_id_type=MESH
        )

    def send(src, dst, group, peer, rsem=None):
        copy_of(src, dst, out_sems.at[group], in_sems.at[group] if rsem is None else rsem, peer).start()

    def arrived(ref, group=None, rsem=None):
        copy_of(ref, ref, out_sems.at[0], in_sems.at[group] if rsem is None else rsem, other).wait_recv()

    def sent(ref, group):
        copy_of(ref, ref, out_sems.at[group], in_sems.at[group], other).wait_send()

    loads = {}

    def load(name, src, dst):
        copy = pltpu.make_async_copy(src, dst, in_sem.at[len(loads)])
        copy.start()
        loads[name] = copy

    def load_chunk(c):
        ks = pl.ds(KAT[c], KAT[c + 1] - KAT[c])
        load(f"fk{c}", fk_hbm.at[ks], fk.at[ks])
        load(f"fv{c}", fv_hbm.at[ks], fv.at[ks])
        load(f"x{c}", x_hbm.at[:, ks], xs.at[:, ks])

    load_chunk(0)
    load("wk", wk_hbm, wk)
    load("wv", wv_hbm, wv)
    for c in range(1, KCHUNKS):
        load_chunk(c)
    load("ck", ck_hbm, cs_k)
    load("cv", cv_hbm, cs_v)
    moments_sem = in_sem.at[len(loads)]
    for src, dst in (
        (m1k_hbm, 0), (m1v_hbm.at[:, pl.ds(0, 128)], 1), (m1v_hbm.at[:, pl.ds(128, 128)], 2),
        (m2k_hbm, 3), (m2v_hbm.at[:, pl.ds(0, 128)], 4), (m2v_hbm.at[:, pl.ds(128, 128)], 5),
    ):
        pltpu.make_async_copy(src, mm.at[dst], moments_sem).start()

    barrier = pltpu.get_barrier_semaphore()

    def greet(peer):
        pl.semaphore_signal(barrier, inc=1, device_id=peer, device_id_type=MESH)

    for tp in (first, second):
        for d in range(1, NZ):
            greet(zpeer(d, tp))
        for d in range(1, NY):
            greet(ypeer(d, tp))
    greet(other)

    @pl.when(adder)
    def _():
        for d in range(1, NX):
            greet((z, y, lax.rem(t + 2 * d, NT)))

    def basis_chunk(c):
        ks = slice(KAT[c], KAT[c + 1])
        for name in ("fk", "fv", "x"):
            loads[f"{name}{c}"].wait()
        xc = xs[:, ks]
        for f, cols in ((fk, slice(0, RK)), (fv, slice(RK, RK + RV))):
            term = jnp.dot(xc, f[ks, :], preferred_element_type=jnp.float32)
            if c == 0:
                basis[:, cols] = term
            else:
                basis[:, cols] += term

    basis_chunk(0)
    loads["wk"].wait()
    loads["wv"].wait()
    kg[core, NEAR, y] = wk[...].astype(jnp.bfloat16)
    vg[core, z, NEAR_Y] = wv[...].astype(jnp.bfloat16)

    @pl.when(mover)
    def _():
        pl.semaphore_wait(barrier, 2 * (NZ - 1 + NY - 1) + 1)

    @pl.when(adder)
    def _():
        pl.semaphore_wait(barrier, 2 * (NZ - 1 + NY - 1) + 1 + NX - 1)
        send(vg.at[1, z, NEAR_Y], vg.at[1, z, NEAR_Y], VALUE_TWIN, other)
        send(kg.at[1, NEAR, y], kg.at[1, NEAR, y], KEY_TWIN, other)

    for d in NEAR_FIRST_Y:
        slot = (NEAR_Y - d) % NY
        send(
            vg.at[core, z, NEAR_Y], vg.at[core, z, slot], VALUE if slot < NY // 2 else VALUE_FAR, ypeer(d, first)
        )
    for d in FAR_Z:
        send(kg.at[core, NEAR, y], kg.at[core, (NEAR - d) % NZ, y], KEY, zpeer(d, first))
    for c in range(1, KCHUNKS):
        basis_chunk(c)

    slots = [lax.rem(i - z + NZ + NEAR, NZ) for i in range(NZ)]
    near, beyond = pl.ds(0, NZ // 2), pl.ds(NZ // 2, NZ // 2)

    loads["ck"].wait()
    loads["cv"].wait()
    dims = (((0,), (0,)), ((), ()))
    for cols, cot, outs in (
        (slice(0, RK), cs_k, slice(0, KC)),
        (slice(RK, RK + RV), cs_v, slice(KC, NC)),
    ):
        b = basis[:, cols]
        upper = b.astype(jnp.bfloat16)
        lower = (b - upper.astype(jnp.float32)).astype(jnp.bfloat16)
        p = lax.dot_general(upper, cot[...], dims, preferred_element_type=jnp.float32)
        p += lax.dot_general(lower, cot[...], dims, preferred_element_type=jnp.float32)
        for b in range(NY):
            for i in range(outs.start // 128, NZ):
                if outs.start <= 128 * (i % 3) < outs.stop:
                    at = ROWS * b + 8 * (i // 3)
                    lanes = 128 * (i % 3) - outs.start
                    piece = p[at : at + 8, lanes : lanes + 128]
                    part[b, slots[i]] = piece
                    rs1_send[b, slots[i]] = piece.astype(jnp.bfloat16)

    for tiles, group in ((beyond, RS_REP_FAR), (near, RS_REP)):
        for d in FAR_Y:
            peer = ypeer(d, second)
            send(rs1_send.at[peer[1], tiles], rs1_recv.at[core, d - 1, tiles], group + core, peer)

        @pl.when(mover)
        def _():
            send(rs1_send.at[y, tiles], rs1_recv.at[0, NY - 1, tiles], group, other)

    pltpu.make_async_copy(mm, mm, moments_sem).wait()
    my_rows = pl.ds(pl.multiple_of(ROWS * y, ROWS), ROWS)

    gather, gather_last = gather_rows(
        z, y, kg, vg, krr, vrr, send, arrived, in_sems, zpeer, ypeer, first, second, other
    )

    @pl.when(mover)
    def _():
        send(mm.at[:, my_rows], twin_mm, MOMENTS_TWIN, other)
        gather()

    def normed_of(proj, first_old, second_old):
        first_new = first_decay * first_old + (1.0 - first_decay) * proj
        second_new = second_decay * second_old + (1.0 - second_decay) * proj * proj
        return first_new, second_new, first_new / (jnp.sqrt(second_new) + epsilon)

    def exchanges():
        for tiles, group, order in (
            (beyond, RS_REP_FAR, (6, 5, 7, 4, 8, 9)), (near, RS_REP, (3, 2, 10, 1, 11, 0)),
        ):
            arrived(rs1_recv.at[0, :, tiles], group)
            arrived(rs1_recv.at[1, pl.ds(0, NY - 1), tiles], group + 1)
            for d in order:
                slot = (d + NEAR) % NZ
                for c in range(2):
                    total = part[y, slot] if c else rs1_recv[0, NY - 1, slot].astype(jnp.float32)
                    for i in range(NY - 1):
                        total += rs1_recv[c, i, slot].astype(jnp.float32)
                    rs2_send[slot, c] = total
            for d in order:
                if d:
                    send(rs2_send.at[(d + NEAR) % NZ], rs2_recv.at[d - 1], RS_FS, zpeer(d, t))

        arrived(twin_mm, MOMENTS_TWIN)
        tile = rs2_send[NEAR]
        arrived(rs2_recv, RS_FS)
        for d in range(1, NZ):
            tile += rs2_recv[d - 1]
        ag[y, NEAR] = tile
        for d in FAR_Z:
            slot = (NEAR - d) % NZ
            send(ag.at[y, NEAR], ag.at[y, slot], AG_FS if slot < NZ // 2 else AG_FS_FAR, zpeer(d, t))

        def ag_send(ref, hops, rsem=None):
            send(ref, ref, AG_REP, ypeer(NY + hops, t), rsem)

        def ag_own(p, tiles):
            for hops, which in ((2, 0), (-2, 1)):
                ag_send(ag.at[y, tiles], hops, a2r.at[which, p])
            for hops in (1, -1):
                ag_send(ag.at[y, tiles], hops)

        def hand_over(block):
            send(ag.at[block, :, 0], ag.at[block, :, 0], AG_TWIN, other)

        def ag_pass(p, tiles):
            for hops, which in ((1, 0), (-1, 1)):
                ref = ag.at[lax.rem(y + NY - 2 * hops, NY), tiles]
                arrived(ref, rsem=a2r.at[which, p])
                ag_send(ref, hops)
                if which == p:
                    ag_send(ref, 2 * hops)

        arrived(ag.at[y, pl.ds(0, NZ // 2 - 1)], AG_FS)
        ag_own(0, near)
        arrived(ag.at[y, beyond], AG_FS_FAR)

        squares = jnp.zeros((8, 128), jnp.float32)
        for i in range(NZ):
            g, r = i % 3, 8 * (i // 3)
            at = pl.ds(pl.multiple_of(ROWS * y + r, 8), 8)
            n = normed_of(ag[y, slots[i], 1], mm[g, at], mm[3 + g, at])[2]
            squares += n * n
            n = normed_of(ag[y, slots[i], 0], twin_mm[g, r : r + 8], twin_mm[3 + g, r : r + 8])[2]
            squares += n * n
        qy[y] = squares
        for d in FAR_Y:
            send(qy.at[y], qy.at[y], SQ_REP, ypeer(d, t))
        ag_own(1, beyond)
        hand_over(y)

        ag_pass(0, near)

        arrived(qy.at[pl.ds(0, NY - 1)], SQ_REP)
        squares = qy[0]
        for i in range(1, NY):
            squares += qy[i]
        qt[x] = squares
        for d in range(1, NX):
            send(qt.at[x], qt.at[x], SQ_TP, (z, y, lax.rem(t + 2 * d, NT)))

        ag_pass(1, beyond)
        for hops in (2, -2):
            hand_over(lax.rem(y + NY + hops, NY))

        arrived(qt.at[pl.ds(0, NX - 1)], SQ_TP)
        squares = qt[0]
        for i in range(1, NX):
            squares += qt[i]
        total_sq[...] = squares
        send(total_sq, total_sq, SQ_TWIN, other)

        arrived(ag.at[pl.ds(0, NY - 3)], AG_REP)
        for hops in (1, -1, 3, -3, 4):
            hand_over(lax.rem(y + NY + hops, NY))

        sent(rs2_recv, RS_FS)
        sent(ag.at[y, pl.ds(0, NZ // 2 - 1)], AG_FS)
        sent(ag.at[y, beyond], AG_FS_FAR)
        sent(ag.at[pl.ds(0, NY - 1)], AG_REP)
        sent(qy.at[pl.ds(0, NY - 1)], SQ_REP)
        sent(qt.at[pl.ds(0, NX - 1)], SQ_TP)

    pl.when(adder)(exchanges)

    @pl.when(mover)
    def _():
        sent(twin_mm, MOMENTS_TWIN)
        arrived(ag.at[:, :, 0], AG_TWIN)
        arrived(total_sq, SQ_TWIN)

    for g in range(3):
        proj = jnp.concatenate([ag[b, slots[3 * i + g], core] for b in range(NY) for i in range(4)], axis=0)
        first_new, second_new, n = normed_of(proj, mm[g], mm[3 + g])
        mm[g] = first_new
        mm[3 + g] = second_new
        upper = n.astype(jnp.bfloat16)
        lower = (n - upper.astype(jnp.float32)).astype(jnp.bfloat16)
        normed[:, 128 * g : 128 * g + 128] = upper
        normed[:, NC + 128 * g : NC + 128 * g + 128] = lower

    squares = total_sq[...]
    whole = jnp.sum(jnp.sum(squares, axis=0, keepdims=True), axis=1, keepdims=True)
    entries = float(RK * DK + RV * DV)
    shrink_out[...] = jnp.broadcast_to(jnp.sqrt(entries / (entries + whole)), (8, 128))

    @pl.when(adder)
    def _():
        arrived(vg.at[1, 0, pl.ds(0, NY - 1)], VALUE_HOME)
        arrived(kg.at[1, pl.ds(0, NZ - 1), 0], KEY_HOME)
        arrived(vg.at[1, pl.ds(0, NZ - 1)], VALUE_RING_HOME)
        arrived(kg.at[1, :, pl.ds(0, NY - 1)], KEY_RING_HOME)
        sent(vg.at[1, z, NEAR_Y], VALUE_TWIN)
        sent(kg.at[1, NEAR, y], KEY_TWIN)
        sent(ag.at[:, :, 0], AG_TWIN)
        sent(total_sq, SQ_TWIN)
        sent(rs1_recv.at[0, pl.ds(0, NY - 1), near], RS_REP + 1)
        sent(rs1_recv.at[0, pl.ds(0, NY - 1), beyond], RS_REP_FAR + 1)

    @pl.when(mover)
    def _():
        gather_last()
        sent(rs1_recv.at[0, :, near], RS_REP)
        sent(rs1_recv.at[0, :, beyond], RS_REP_FAR)
        sent(vg.at[0, 0, pl.ds(0, NY - 1)], VALUE_HOME)
        sent(kg.at[0, pl.ds(0, NZ - 1), 0], KEY_HOME)
        sent(vg.at[0, pl.ds(0, NZ - 2)], VALUE_RING_HOME)
        sent(kg.at[0, :, pl.ds(0, NY - 2)], KEY_RING_HOME)
        sent(kg.at[:, :, pl.ds(0, NY - 1)], KEY_RING)
        sent(vg.at[:, pl.ds(0, NZ - 1)], VALUE_RING)

    sent(vg.at[0, 0, pl.ds(0, NY // 2 - 1)], VALUE)
    sent(vg.at[0, 0, pl.ds(0, NY // 2)], VALUE_FAR)
    sent(kg.at[0, pl.ds(0, NZ - 1), 0], KEY)


def gather_rows(z, y, kg, vg, krr, vrr, send, arrived, in_sems, zpeer, ypeer, mine, twin, other):
    def ring(block, chunks, me, n, peer_of, group, home, rsem):
        steps = n // 2

        def owner_of(direction, hops):
            return lax.rem(me + (n - hops if direction == 0 else hops), n)

        def carries(direction, s, c):
            return s < steps or (c < chunks // 2) == (direction == 0)

        def put(direction, s, c):
            owner, hop = owner_of(direction, s - 1), 1 if direction == 0 else n - 1
            rs = rsem.at[direction, s - 1, c]
            if s < steps:
                ref = block(slice(None), owner, c)
                send(ref, ref, group, peer_of(hop, mine), rs)
            else:
                for h, tp, sem in ((0, mine, rs), (1, twin, in_sems.at[home])):
                    send(block(h, owner, c), block(h, owner, c), group, peer_of(hop, tp), sem)

        def take(direction, s, c):
            owner = owner_of(direction, s)
            rs = rsem.at[direction, s - 1, c]
            if s == steps:
                arrived(block(0, owner, c), rsem=rs)
                return
            arrived(block(slice(None), owner, c), rsem=rs)
            if carries(direction, s + 1, c):
                put(direction, s + 1, c)
            send(block(1, owner, c), block(1, owner, c), home, other)

        def round_(s, chosen=range(chunks)):
            for c in chosen:
                for direction in range(2):
                    if s == 0:
                        put(direction, 1, c)
                    elif carries(direction, s, c):
                        take(direction, s, c)

        return round_

    kround = ring(
        lambda h, o, c: kg.at[h, pl.ds(c * (NZ // KCH), NZ // KCH), o],
        KCH, y, NY, ypeer, KEY_RING, KEY_RING_HOME, krr,
    )
    vround = ring(
        lambda h, o, c: vg.at[h, o, pl.ds(c * (NY // VCH), NY // VCH)],
        VCH, z, NZ, zpeer, VALUE_RING, VALUE_RING_HOME, vrr,
    )
    lower, upper = range(VCH // 2), range(VCH // 2, VCH)

    def home(ref, group):
        send(ref, ref, group, other)

    def gather():
        arrived(vg.at[1, z, NEAR_Y], VALUE_TWIN)
        arrived(vg.at[:, z, pl.ds(0, NY // 2 - 1)], VALUE)
        vround(0, lower)
        arrived(vg.at[:, z, pl.ds(NY // 2, NY // 2)], VALUE_FAR)
        vround(0, upper)
        for at, count in ((0, NEAR_Y), (NEAR_Y + 1, NY - NEAR_Y - 1)):
            home(vg.at[1, z, pl.ds(at, count)], VALUE_HOME)
        vround(1, lower)
        arrived(kg.at[1, NEAR, y], KEY_TWIN)
        arrived(kg.at[:, pl.ds(0, NZ - 1), y], KEY)
        kround(0)
        for at, count in ((0, NEAR), (NEAR + 1, NZ - NEAR - 1)):
            home(kg.at[1, pl.ds(at, count), y], KEY_HOME)
        vround(1, upper)
        vround(2, lower)
        kround(1)
        vround(2, upper)
        vround(3, lower)
        kround(2)
        vround(3, upper)
        vround(4, lower)
        vround(4, upper)
        vround(5, lower)
        vround(5, upper)
        kround(3)

    def gather_last():
        vround(6)
        kround(4)

    return gather, gather_last


def finish(
    kg, vg, fk, fv, wk, wv, mm, normed, shrink_in,
    wkn_hbm, wvn_hbm, m1kn_hbm, m2kn_hbm, m1vn_hbm, m2vn_hbm, sk_hbm, sv_hbm, kcopy_hbm, vcopy_hbm,
    kout, vout, ok, ov, osk, osv, out_sem,
):
    z, y, core = lax.axis_index("fs"), lax.axis_index("rep"), lax.rem(lax.axis_index("tp"), 2)
    outs = []

    def store(src, dst):
        copy = pltpu.make_async_copy(src, dst, out_sem.at[len(outs)])
        copy.start()
        outs.append(copy)

    for src, dst in (
        (0, m1kn_hbm), (1, m1vn_hbm.at[:, pl.ds(0, 128)]), (2, m1vn_hbm.at[:, pl.ds(128, 128)]),
        (3, m2kn_hbm), (4, m2vn_hbm.at[:, pl.ds(0, 128)]), (5, m2vn_hbm.at[:, pl.ds(128, 128)]),
    ):
        store(mm.at[src], dst)

    shrink = shrink_in[0:1, 0:1]

    def steps_of(rows, parts):
        key_step = value_step = 0.0
        for at in parts:
            key_step += jnp.dot(fk[rows, :], normed[:, at : at + KC], preferred_element_type=jnp.float32)
            value_step += jnp.dot(fv[rows, :], normed[:, at + KC : at + NC], preferred_element_type=jnp.float32)
        return shrink * key_step, shrink * value_step

    blocks = STEP // 256
    for b in range(D // STEP):
        rows = slice(b * STEP, b * STEP + STEP)
        key_step, value_step = steps_of(rows, (0,))
        kw = jnp.concatenate(
            [
                kg[core, lax.rem(blocks * b + i - z + NZ + NEAR, NZ)].reshape(256, KC)
                for i in range(blocks)
            ],
            axis=0,
        ).astype(jnp.float32)
        kout[rows, :] = (kw - learn_rate * key_step).astype(jnp.bfloat16)
        vw = jnp.concatenate(
            [vg[core, blocks * b + i, lax.rem(j - y + NY + NEAR_Y, NY)] for i in range(blocks) for j in range(NY)], axis=0
        ).astype(jnp.float32)
        vout[rows, :] = (vw - learn_rate * value_step).astype(jnp.bfloat16)
        store(kout.at[pl.ds(b * STEP, STEP)], kcopy_hbm.at[pl.ds(b * STEP, STEP)])
        store(vout.at[pl.ds(b * STEP, STEP)], vcopy_hbm.at[pl.ds(b * STEP, STEP)])

    key_step, value_step = steps_of(pl.ds(pl.multiple_of((z * NY + y) * ROWS, ROWS), ROWS), (0, NC))
    osk[...] = key_step
    osv[...] = value_step
    ok[...] = wk[...] - learn_rate * key_step
    ov[...] = wv[...] - learn_rate * value_step
    store(osk, sk_hbm)
    store(osv, sv_hbm)
    store(ok, wkn_hbm)
    store(ov, wvn_hbm)
    for copy in outs:
        copy.wait()


def body(*args):
    f32, bf16 = jnp.float32, jnp.bfloat16
    V, S = pltpu.VMEM, pltpu.SemaphoreType.DMA
    outs = [
        ((ROWS, KC), f32), ((ROWS, VC), f32), ((RK, KC), f32), ((RK, KC), f32), ((RV, VC), f32), ((RV, VC), f32),
        ((ROWS, KC), f32), ((ROWS, VC), f32), ((D, KC), bf16), ((D, VC), bf16),
    ]
    held = [
        V((2, NZ, NY, ROWS, KC), bf16), V((2, NZ, NY, ROWS, VC), bf16), V((D, RK), bf16), V((D, RV), bf16),
        V((ROWS, KC), f32), V((ROWS, VC), f32), V((6, RK, 128), f32), V((RK, 2 * NC), bf16), V((8, 128), f32),
    ]
    held_specs = [pl.BlockSpec(memory_space=V)] * len(held)
    middle = pl.pallas_call(
        kernel,
        name="projected_update",
        out_shape=held,
        in_specs=[pl.BlockSpec(memory_space=pltpu.HBM)] * 11,
        out_specs=held_specs,
        scratch_shapes=[
            V((TOK, D), bf16), V((TOK, KC), bf16), V((TOK, VC), bf16),
            V((TOK, RK + RV), f32), V((NY, NZ, 8, 128), f32), V((NY, NZ, 8, 128), bf16), V((2, NY, NZ, 8, 128), bf16),
            V((NZ, 2, 8, 128), f32), V((NZ - 1, 2, 8, 128), f32), V((NY, NZ, 2, 8, 128), f32),
            V((NX, 8, 128), f32), V((NY, 8, 128), f32), V((8, 128), f32), V((6, ROWS, 128), f32),
            S((2 + 3 * KCHUNKS + 2 + 1,)), S((GROUPS,)), S((GROUPS,)), S((2, 2)),
            S((2, NY // 2, KCH)), S((2, NZ // 2, VCH)),
        ],
        compiler_params=pltpu.CompilerParams(collective_id=0, has_side_effects=True, vmem_limit_bytes=VMEM_MAIN),
    )(*args)
    return pl.pallas_call(
        finish,
        name="finish",
        out_shape=[jax.ShapeDtypeStruct(s, dt) for s, dt in outs],
        in_specs=held_specs,
        out_specs=[pl.BlockSpec(memory_space=pltpu.HBM)] * len(outs),
        scratch_shapes=[
            V((D, KC), bf16), V((D, VC), bf16),
            V((ROWS, KC), f32), V((ROWS, VC), f32), V((ROWS, KC), f32), V((ROWS, VC), f32),
            S((10 + 2 * (D // STEP),)),
        ],
        compiler_params=pltpu.CompilerParams(vmem_limit_bytes=16 << 20),
    )(*middle)


def solution(mesh):
    tokens, rows, cols = P(("fs", "rep"), None), P(("fs", "rep"), "tp"), P(None, "tp")
    in_specs = (tokens, rows, rows, P(), P(), rows, rows, cols, cols, cols, cols)
    out_specs = (rows, rows, cols, cols, cols, cols, rows, rows, cols, cols)
    return jax.shard_map(body, mesh=mesh, in_specs=in_specs, out_specs=out_specs, check_vma=False)
```

time: 55.4 us -> 53.8 us (0.971)
  Pallas kernels: 54.7 us -> 53 us
    pallas_call x1, Pallas kernels: 52.6 us -> 51 us  [body(): pl.pallas_call(kernel, name='projected_update', out_shape=held, in_specs=...]
where the time goes in v4:
time: 53.8 us; the launch traced here: 53.7 us
  Pallas kernels  53 us (99%)
  between operations  0.65 us (1%)
    pallas_call x1, Pallas kernels, body(): pl.pallas_call(kernel, name='projected_update', out_shape=held, in_specs=...  51 us
    pallas_call x1, Pallas kernels, body(): pl.pallas_call(finish, name='finish', out_shape=[jax.ShapeDtypeStruct(s,...  1.97 us

profile of v4, /device:TPU:1, one launch (start us, length us, event | category | flops | bytes accessed | tf_op | source)
XLA Modules:
  0.0 53.7 jit_solution(12596743449588910317)
XLA Ops:
  0.6 51.0 %projected_update.1 = (bf16[2,12,8,32,128]{4,3,2,1,0:T(8,128)(2,1)S(1)}, bf16[2,12,8,32,256]{4,3,2,1,0:T(8,128)(2,1)S(1)}, bf16[3072,256]{1,0:T(8,128)(2,1)S(1)}...) custom-call(bf16[640,3072]{1,0:T(8,128)(2,1)} %x_hbm.1, ...), custom_call_target="tpu_custom_call" | custom-call | tf_op jit(solution)/shard_map/projected_update/pallas_call | solution.py:513
  51.7 2.0 %finish.1 = (f32[32,128]{1,0:T(8,128)}, f32[32,256]{1,0:T(8,128)}, f32[256,128]{1,0:T(8,128)}, f32[256,128]{1,0:T(8,128)}, f32[256,256]{1,0:T(8,128)}, /*index=5...) custom-call(bf16[2,12,8,32,128]{4,3,2,1,0:T(8,128)(2,1)S(1)} %get-tu, ...), custom_call_target="tpu_custom_call" | custom-call | tf_op jit(solution)/shard_map/finish/pallas_call | solution.py:529
